TPU v7x, 32 devices: a whole 2x2x4 slice. The times are simulated.
32 devices in a mesh: grp: 2 (over y), sp: 4 (over z), tp: 4 (over x, core).
Axes of the slice: x: 2, y: 2, z: 4, core: 2. Of those that a mesh axis runs over, the one named last changes fastest.
Arguments:
- queries: bfloat16 [4096, 1024], P(('grp', 'sp'), 'tp'), parts along dimension 0, may hold values from -120 to 120
- keys: bfloat16 [4096, 256], P(('grp', 'sp')), parts along dimension 0, may hold values from -6 to 6
- values: bfloat16 [4096, 256], P(('grp', 'sp')), parts along dimension 0, may hold values from -6 to 6
- sink: float32 [8], P('tp'), may hold values from 1 to 5
- resid: bfloat16 [4096, 2048], P(('grp', 'sp')), parts along dimension 0, may hold values from -100 to 100
- out_proj: bfloat16 [1024, 2048], P(None, 'tp'), may hold values from -1.5 to 1.5
- norm_gain: float32 [2048], replicated, may hold values from 0.1 to 1.9
- w_gate: bfloat16 [2048, 6144], P('sp', 'tp'), may hold values from -0.125 to 0.125
- w_up: bfloat16 [2048, 6144], P('sp', 'tp'), may hold values from -0.125 to 0.125
- conv_w: float32 [3, 6144], P(None, 'tp'), may hold values from -3 to 3
- conv_b: float32 [6144], P('tp'), may hold values from -3 to 3
- w_down: bfloat16 [6144, 2048], P('tp', 'sp'), may hold values from -0.21875 to 0.21875
Outputs:
- layer_out: bfloat16 [4096, 2048], P(('grp', 'sp'), 'tp'), parts along dimension 0
There are 2 independent parts, one for each index of `grp`. A program takes and returns all parts, laid end to end along the dimension named above; an argument that names none is the same for every part. Nothing has to cross between parts.
All inputs are finite; a program needn't handle non-finite values.
Results may differ from a plain program's by a relative error of at most 0.015.
Values may be sent and summed in bfloat16 or wider, within the bound.
A program may use at most 64 MiB of HBM per device.

v0:
```python
import functools

import jax
import jax.numpy as jnp
from jax import lax
from jax.experimental import pallas as pl
from jax.experimental.pallas import tpu as pltpu
from jax.sharding import PartitionSpec as P

H = 8
KVH = 2
HD = 128
WINDOW = 128
CONV = 3


def with_halo(cells, sides, width):
    for axis, dim in sides:
        count = lax.axis_size(axis)
        ends = count - 1
        head = lax.slice_in_dim(cells, 0, width, axis=dim)
        tail = lax.slice_in_dim(cells, cells.shape[dim] - width, cells.shape[dim], axis=dim)
        cells = jnp.concatenate(
            [
                lax.ppermute(tail, axis, [(i, (i + 1) % count) for i in range(ends)]),
                cells,
                lax.ppermute(head, axis, [((i + 1) % count, i) for i in range(ends)]),
            ],
            axis=dim,
        )
    return cells


def shards(
    queries, keys, values, sink, resid, out_proj, norm_gain, w_gate, w_up, conv_w, conv_b, w_down
):
    tokens = queries.shape[0]
    width = resid.shape[1]
    heads_here = sink.shape[0]
    group = H // KVH
    scale = HD ** (-0.5)
    first_head = lax.axis_index("tp") * heads_here
    kv_head = first_head // group
    own_keys = lax.dynamic_slice_in_dim(keys, kv_head * HD, HD, 1)
    own_values = lax.dynamic_slice_in_dim(values, kv_head * HD, HD, 1)
    extended = with_halo(jnp.stack([own_keys, own_values]), (("sp", 1),), WINDOW)
    ext_keys = extended[0]
    ext_values = extended[1]
    span = tokens + 2 * WINDOW
    q_heads = queries.reshape(tokens, heads_here, HD)
    scores = (
        jnp.einsum("qhd,kd->hqk", q_heads, ext_keys, preferred_element_type=jnp.float32) * scale
    )
    offset = lax.axis_index("sp") * tokens
    q_pos = offset + jnp.arange(tokens, dtype=jnp.int32)[:, None]
    k_pos = offset - WINDOW + jnp.arange(span, dtype=jnp.int32)[None, :]
    seq_total = tokens * lax.axis_size("sp")
    valid = (jnp.abs(q_pos - k_pos) <= WINDOW) & (k_pos >= 0) & (k_pos < seq_total)
    scores = jnp.where(valid[None], scores, jnp.float32(-1e30))
    sink_col = sink[:, None]
    top = jnp.maximum(jnp.max(scores, axis=-1), sink_col)
    expo = jnp.exp(scores - top[..., None])
    total = jnp.sum(expo, axis=-1) + jnp.exp(sink_col - top)
    weights = (expo / total[..., None]).astype(jnp.bfloat16)
    heads_out = jnp.einsum("hqk,kd->qhd", weights, ext_values, preferred_element_type=jnp.float32)
    heads_out = heads_out.astype(jnp.bfloat16).reshape(tokens, heads_here * HD)
    all_heads = lax.all_gather(heads_out, "tp", axis=1, tiled=True)
    cols = width // lax.axis_size("tp")
    col_start = lax.axis_index("tp") * cols
    full_proj = lax.all_gather(out_proj, "tp", axis=1, tiled=True)
    summed = resid.astype(jnp.float32) + jnp.dot(
        all_heads, full_proj, preferred_element_type=jnp.float32
    )
    mean = jnp.mean(summed, axis=-1, keepdims=True)
    msq = jnp.mean(summed * summed, axis=-1, keepdims=True)
    normed_full = ((summed - mean) * lax.rsqrt(msq - mean * mean + 1e-05) * norm_gain).astype(
        jnp.bfloat16
    )
    normed_own = lax.dynamic_slice_in_dim(normed_full, col_start, cols, 1)
    gate_acc = jnp.dot(
        normed_full,
        lax.all_gather(w_gate, "sp", axis=0, tiled=True),
        preferred_element_type=jnp.float32,
    )
    up_acc = jnp.dot(
        normed_full,
        lax.all_gather(w_up, "sp", axis=0, tiled=True),
        preferred_element_type=jnp.float32,
    )
    gate_pre = gate_acc.astype(jnp.bfloat16)
    up_part = up_acc.astype(jnp.bfloat16)
    padded = with_halo(gate_pre, (("sp", 0),), CONV // 2)
    conv = conv_b
    for tap in range(CONV):
        conv = conv + padded[tap : tap + tokens].astype(jnp.float32) * conv_w[tap]
    act = (jax.nn.silu(conv) * up_part.astype(jnp.float32)).astype(jnp.bfloat16)
    terms = jnp.dot(
        act, lax.all_gather(w_down, "sp", axis=1, tiled=True), preferred_element_type=jnp.float32
    )
    ffn_own = lax.psum_scatter(
        terms.astype(jnp.bfloat16), "tp", scatter_dimension=1, tiled=True
    ).astype(jnp.float32)
    return (normed_own.astype(jnp.float32) + ffn_own).astype(jnp.bfloat16)


CHUNKS = 2
CROSSED = 1
PAD = 8
EDGE = 16
BF16 = jnp.bfloat16
F32 = jnp.float32


def layer_kernel(
    sizes,
    q_ref, k_ref, v_ref, sink_ref, resid_ref, proj_ref, gain_ref, wg_ref, wu_ref, cw_ref, cb_ref, wd_ref,
    out_ref,
    kv_ext, proj_all, mixed, summed, normed, wg_all, wu_all, wd_all, gate, up, edge, halo, act, terms, parts,
    pair_in, ret_out, ret_in,
    halo_send, halo_recv, z_recv, z_send, y_recv, y_send,
    proj_send, proj_recv, mix_send, mix_recv, norm_send, norm_recv, edge_send, edge_recv,
    term_send, term_recv, pair_send, pair_recv, ret_send, ret_recv,
):
    groups, n, tps = sizes
    g = lax.axis_index("grp")
    s = lax.axis_index("sp")
    t = lax.axis_index("tp")
    tokens, width = resid_ref.shape
    heads_here = sink_ref.shape[0]
    cols = proj_ref.shape[1]
    depth = wg_ref.shape[0]
    hidden = wg_ref.shape[1]
    rows2 = 2 * tokens
    has_left, has_right = s > 0, s < n - 1
    inner = has_left & has_right
    outer = jnp.logical_not(inner)
    low = s < n // 2
    inward = 1 - 2 * (s // (n // 2))
    base = pl.multiple_of(lax.rem(s, 2) * tokens, tokens)
    other_base = pl.multiple_of((1 - lax.rem(s, 2)) * tokens, tokens)
    core_peer = t + 1 - 2 * lax.rem(t, 2)
    chip_peer = lax.rem(t + 2, tps)
    own = (wg_ref, wu_ref, wd_ref)
    full = (wg_all, wu_all, wd_all)

    def remote(src, dst, send, recv, to):
        return pltpu.make_async_remote_copy(
            src_ref=src, dst_ref=dst, send_sem=send, recv_sem=recv,
            device_id=to, device_id_type=pl.DeviceIdType.MESH,
        )

    barrier = pltpu.get_barrier_semaphore()

    def greet(to):
        pl.semaphore_signal(barrier, inc=1, device_id=to, device_id_type=pl.DeviceIdType.MESH)

    @pl.when(has_left)
    def _():
        greet({"sp": s - 1})

    @pl.when(has_right)
    def _():
        greet({"sp": s + 1})

    for j in range(1, groups):
        greet({"grp": lax.rem(g + j, groups)})
    for j in range(1, tps):
        greet({"tp": lax.rem(t + j, tps)})
    along = jnp.minimum(s, 1) + jnp.minimum(n - 1 - s, 1)
    pl.semaphore_wait(barrier, along + groups - 1 + tps - 1)

    kv_head = (t * heads_here) // (H // KVH)
    kv_cols = pl.ds(pl.multiple_of(kv_head * HD, HD), HD)

    def halo_copy(i, to_left):
        ref = (k_ref, v_ref)[i]
        if to_left:
            return remote(ref.at[pl.ds(0, WINDOW), kv_cols], kv_ext.at[i, pl.ds(WINDOW + tokens, WINDOW)],
                          halo_send.at[i, 0], halo_recv.at[i, 0], {"sp": s - 1})
        return remote(ref.at[pl.ds(tokens - WINDOW, WINDOW), kv_cols], kv_ext.at[i, pl.ds(0, WINDOW)],
                      halo_send.at[i, 1], halo_recv.at[i, 1], {"sp": s + 1})

    def rows_of(m, part, c):
        step = own[m].shape[0] // (groups * CHUNKS)
        return pl.ds(pl.multiple_of((part * CHUNKS + c) * step, EDGE), step)

    def hop(m, src_slot, dst_slot, j, c):
        part = lax.rem(g + j, groups)
        rows = rows_of(m, part, c)
        src = own[m].at[rows] if src_slot is None else full[m].at[src_slot, rows]
        return remote(src, full[m].at[dst_slot, rows], z_send.at[m, 0 if src_slot is None else 1, j, c],
                      z_recv.at[m, dst_slot, j, c], {"sp": s + inward})

    def cross(m, slot, c, j):
        rows = rows_of(m, g, c)
        return remote(full[m].at[slot, rows], full[m].at[slot, rows], y_send.at[m, slot, c, j],
                      y_recv.at[m, slot, c, j], {"grp": lax.rem(g + j, groups)})

    def cross_arrival(m, slot, c, j):
        rows = rows_of(m, lax.rem(g + groups - j, groups), c)
        return remote(full[m].at[slot, rows], full[m].at[slot, rows], y_send.at[m, slot, c, j],
                      y_recv.at[m, slot, c, j], {"grp": lax.rem(g + j, groups)})

    pieces = [(m, c) for m in range(3) for c in range(CHUNKS)]
    crossed = pieces[:CROSSED]
    direct = [(m, c, j) for m, c in pieces[CROSSED:] for j in range(1, groups)]

    def spread(src, ref, send, recv, step):
        origin = (t, t, chip_peer)[step]
        return remote(src if step < 2 else ref.at[origin], ref.at[origin], send.at[step], recv.at[step],
                      {"tp": (core_peer, chip_peer, core_peer)[step]})

    def spread_arrival(src, ref, send, recv, step):
        origin = (core_peer, chip_peer, lax.rem(core_peer + 2, tps))[step]
        return remote(src, ref.at[origin], send.at[step], recv.at[step],
                      {"tp": (core_peer, chip_peer, core_peer)[step]})

    proj_args = (proj_ref, proj_all, proj_send, proj_recv)
    mix_args = (mixed.at[t], mixed, mix_send, mix_recv)

    @pl.when(has_left)
    def _():
        for i in range(2):
            halo_copy(i, True).start()

    @pl.when(has_right)
    def _():
        for i in range(2):
            halo_copy(i, False).start()

    @pl.when(outer)
    def _():
        for m, c in pieces:
            hop(m, None, 0, 0, c).start()

    @pl.when(inner)
    def _():
        for m, c in pieces[:2 * CHUNKS]:
            hop(m, None, 1, 0, c).start()

    for step in (1, 0):
        spread(*proj_args, step).start()

    for i, ref in enumerate((k_ref, v_ref)):
        kv_ext[i, pl.ds(WINDOW, tokens), :] = ref[:, kv_cols]

    @pl.when(jnp.logical_not(has_left))
    def _():
        kv_ext[:, pl.ds(0, WINDOW), :] = jnp.zeros((2, WINDOW, HD), BF16)

    @pl.when(jnp.logical_not(has_right))
    def _():
        kv_ext[:, pl.ds(WINDOW + tokens, WINDOW), :] = jnp.zeros((2, WINDOW, HD), BF16)

    @pl.when(has_right)
    def _():
        for i in range(2):
            halo_copy(i, True).wait_recv()

    @pl.when(has_left)
    def _():
        for i in range(2):
            halo_copy(i, False).wait_recv()

    span = 3 * WINDOW
    seq_total = tokens * n

    @pl.loop(0, tokens // WINDOW)
    def _(b):
        start = pl.multiple_of(b * WINDOW, WINDOW)
        row = lax.broadcasted_iota(jnp.int32, (WINDOW, span), 0)
        col = lax.broadcasted_iota(jnp.int32, (WINDOW, span), 1)
        k_pos = s * tokens + start - WINDOW + col
        valid = (jnp.abs(row + WINDOW - col) <= WINDOW) & (k_pos >= 0) & (k_pos < seq_total)
        kb = kv_ext[0, pl.ds(start, span), :]
        vb = kv_ext[1, pl.ds(start, span), :]
        for h in range(heads_here):
            qb = q_ref[pl.ds(start, WINDOW), h * HD:(h + 1) * HD]
            sc = lax.dot_general(qb, kb, (((1,), (1,)), ((), ())), preferred_element_type=F32) * (HD ** -0.5)
            sc = jnp.where(valid, sc, F32(-1e30))
            sink = sink_ref[h]
            top = jnp.maximum(jnp.max(sc, axis=-1, keepdims=True), sink)
            expo = jnp.exp(sc - top)
            total = jnp.sum(expo, axis=-1, keepdims=True) + jnp.exp(sink - top)
            weights = (expo / total).astype(BF16)
            o = jnp.dot(weights, vb, preferred_element_type=F32)
            mixed[t, pl.ds(start, WINDOW), h * HD:(h + 1) * HD] = o.astype(BF16)

    proj_all[t] = proj_ref[...]
    for step in (1, 0):
        spread(*mix_args, step).start()

    def relay_near(m):
        for c in range(CHUNKS):
            hop(m, None, 0, 0, c).wait_recv()
            hop(m, 0, 2, 0, c).start()
            if (m, c) in crossed:
                for j in range(1, groups):
                    cross(m, 0, c, j).start()
            hop(m, None, 1, 0, c).wait_recv()
            for j in range(1, groups):
                cross(m, 1, c, j).start()

    def relay_far(m):
        for c in range(CHUNKS):
            hop(m, 0, 2, 0, c).wait_recv()
            for j in range(1, groups):
                cross(m, 2, c, j).start()

    @pl.when(inner)
    def _():
        relay_near(0)

    for args in (proj_args, mix_args):
        spread_arrival(*args, 1).wait_recv()
        spread(*args, 2).start()
    for args in (proj_args, mix_args):
        for step in (0, 2):
            spread_arrival(*args, step).wait_recv()
    lanes = mixed.shape[2]
    block = summed.shape[0]
    strip = 64

    @pl.loop(0, tokens // block)
    def _(b):
        rows = pl.ds(pl.multiple_of(b * block, block), block)

        @pl.loop(0, tps)
        def _(i):
            at = pl.ds(pl.multiple_of(i * cols, 128), cols)
            prod = jnp.dot(mixed[0, rows, :], proj_all[i, pl.ds(0, lanes), :], preferred_element_type=F32)
            for u in range(1, tps):
                prod += jnp.dot(mixed[u, rows, :], proj_all[i, pl.ds(u * lanes, lanes), :],
                                preferred_element_type=F32)
            summed[:, at] = resid_ref[rows, at].astype(F32) + prod

        @pl.loop(0, block // strip)
        def _(i):
            at = pl.multiple_of(i * strip, strip)
            x = summed[pl.ds(at, strip), :]
            mean = jnp.mean(x, axis=-1, keepdims=True)
            msq = jnp.mean(x * x, axis=-1, keepdims=True)
            normed[pl.ds(pl.multiple_of(base + b * block + at, strip), strip), :] = (
                (x - mean) * lax.rsqrt(msq - mean * mean + 1e-05) * gain_ref[...]
            ).astype(BF16)

    half = width // 2
    my_half = pl.ds(pl.multiple_of(lax.rem(t, 2) * half, half), half)
    peer_half = pl.ds(pl.multiple_of((1 - lax.rem(t, 2)) * half, half), half)

    def norm_in():
        part = normed.at[pl.ds(base, tokens), my_half]
        return remote(part, part, norm_send.at[0], norm_recv.at[0], {"sp": s + inward})

    def norm_in_arrival():
        part = normed.at[pl.ds(other_base, tokens), my_half]
        return remote(part, part, norm_send.at[0], norm_recv.at[0], {"sp": s + inward})

    def norm_over(of_peer):
        part = normed.at[pl.ds(other_base, tokens), peer_half if of_peer else my_half]
        return remote(part, part, norm_send.at[1], norm_recv.at[1], {"tp": core_peer})

    def ret_copy():
        return remote(ret_out, ret_in, ret_send.at[0], ret_recv.at[0], {"sp": s - inward})

    def edge_copy():
        return remote(edge, halo, edge_send.at[0], edge_recv.at[0], {"sp": s + inward})

    half_rows = tokens // 2
    core = lax.rem(t, 2)
    far_first = (1 - t // 2) * 2

    def is_far(p):
        return (p // 2) != (t // 2)

    def half_of(i, c):
        first = (base if i else other_base) + c * half_rows
        return pl.ds(pl.multiple_of(first, half_rows), half_rows)

    def near_copy(i, u):
        rows = pl.ds(base if i else other_base, tokens)
        return remote(terms.at[core_peer, rows], parts.at[u, rows], term_send.at[core_peer, i],
                      term_recv.at[u, i], {"tp": core_peer})

    def pair_copy(p, i):
        return remote(terms.at[p, half_of(i, 1 - core)], pair_in.at[lax.rem(p, 2), i],
                      pair_send.at[lax.rem(p, 2), i], pair_recv.at[lax.rem(p, 2), i], {"tp": core_peer})

    def far_copy(p, i):
        rows = half_of(i, core)
        return remote(terms.at[p, rows], parts.at[t, rows], term_send.at[p, i], term_recv.at[t, i], {"tp": p})

    def far_arrival(c, i):
        u, rows = far_first + c, half_of(i, c)
        return remote(terms.at[u, rows], parts.at[u, rows], term_send.at[u, i], term_recv.at[u, i], {"tp": u})

    tile = 256
    my_cols = pl.ds(pl.multiple_of(t * cols, 128), cols)

    def arrived(m, slot):
        for c in range(CHUNKS):
            for j in range(1, groups):
                if slot == 0 and (m, c) not in crossed:
                    hop(m, None, 0, j, c).wait_recv()
                else:
                    cross_arrival(m, slot, c, j).wait_recv()

    def gate_up(slot):
        if slot is not None:
            arrived(0, slot)
            arrived(1, slot)
        p = s + {None: 0, 0: -1, 1: 1, 2: 2}[slot] * inward

        @pl.loop(0, hidden // tile)
        def _(i):
            at = pl.ds(pl.multiple_of(i * tile, 128), tile)
            x = normed[:, pl.ds(pl.multiple_of(p * depth, 128), depth)]
            wa = wg_ref[:, at] if slot is None else wg_all[slot, :, at]
            ga = jnp.dot(x, wa, preferred_element_type=F32)
            if slot is None:
                gate[pl.ds(PAD, rows2), at] = ga
            else:
                gate[pl.ds(PAD, rows2), at] += ga
            wb = wu_ref[:, at] if slot is None else wu_all[slot, :, at]
            ub = jnp.dot(x, wb, preferred_element_type=F32)
            if slot is None:
                up[:, at] = ub
            else:
                up[:, at] += ub

    def piece_of(slot):
        return s + {None: 0, 0: -1, 1: 1, 2: 2}[slot] * inward

    def down(slot, i):
        if slot is not None and i == 0:
            arrived(2, slot)
        p = piece_of(slot)
        rows = pl.ds(base if i else other_base, tokens)

        @pl.loop(0, cols // tile)
        def _(k):
            at = pl.ds(pl.multiple_of(k * tile, 128), tile)
            w = wd_ref[:, at] if slot is None else wd_all[slot, :, at]
            terms[p, rows, at] = jnp.dot(act[rows, :], w, preferred_element_type=F32).astype(BF16)

        @pl.when(p == core_peer)
        def _():
            near_copy(i, t).start()

        @pl.when(is_far(p))
        def _():
            pair_copy(p, i).start()

    def settle(slot, i):
        p = piece_of(slot)

        @pl.when(is_far(p))
        def _():
            pair_copy(p, i).wait_recv()
            rows = half_of(i, core)
            both = terms[p, rows, :].astype(F32) + pair_in[lax.rem(p, 2), i].astype(F32)
            terms[p, rows, :] = both.astype(BF16)
            far_copy(p, i).start()

    def finish(i, ref):
        near_copy(i, core_peer).wait_recv()
        for c in range(2):
            rows = half_of(i, c)
            out = normed[rows, my_cols].astype(F32) + terms[t, rows, :].astype(F32)
            out = out + parts[core_peer, rows, :].astype(F32)
            far_arrival(c, i).wait_recv()
            out = out + parts[far_first + c, rows, :].astype(F32)
            ref[pl.ds(c * half_rows, half_rows), :] = out.astype(BF16)

    @pl.when(outer)
    def _():
        norm_in().start()
        for m, c, j in direct:
            hop(m, None, 0, j, c).start()
        ret_copy().wait_recv()
        out_ref[...] = ret_in[...]
        norm_in().wait_send()
        for m, c, j in direct:
            hop(m, None, 0, j, c).wait_send()
        for m, c in pieces:
            hop(m, None, 0, 0, c).wait_send()

    @pl.when(inner)
    def _():
        relay_near(1)
        for m, c in pieces[2 * CHUNKS:]:
            hop(m, None, 1, 0, c).start()
        relay_far(0)
        relay_far(1)
        norm_in_arrival().wait_recv()
        norm_over(False).start()
        relay_near(2)
        norm_over(True).wait_recv()
        gate_up(None)
        gate_up(1)
        gate_up(2)
        relay_far(2)
        gate_up(0)

        at_edge = pl.multiple_of(PAD + (1 - s // (n // 2)) * (rows2 - EDGE), PAD)
        edge[...] = gate[pl.ds(at_edge, EDGE), :].astype(BF16)
        edge_copy().start()
        gate[PAD - 1:PAD, :] = jnp.zeros((1, hidden), F32)
        gate[PAD + rows2:PAD + rows2 + 1, :] = jnp.zeros((1, hidden), F32)
        edge_copy().wait_recv()

        @pl.when(low)
        def _():
            gate[PAD + rows2:PAD + rows2 + 1, :] = halo[...].astype(F32)[0:1, :]

        @pl.when(jnp.logical_not(low))
        def _():
            gate[PAD - 1:PAD, :] = halo[...].astype(F32)[EDGE - 1:EDGE, :]

        @pl.loop(0, hidden // 128)
        def _(i):
            at = pl.ds(pl.multiple_of(i * 128, 128), 128)
            gate[pl.ds(PAD, rows2), at] = gate[pl.ds(PAD, rows2), at].astype(BF16).astype(F32)
            conv = cb_ref[:, at]
            for tap in range(CONV):
                conv = conv + gate[pl.ds(PAD - CONV // 2 + tap, rows2), at] * cw_ref[tap:tap + 1, at]
            silu = conv / (1.0 + jnp.exp(-conv))
            act[:, at] = (silu * up[:, at].astype(BF16).astype(F32)).astype(BF16)

        steps = [(slot, i) for slots in ((None, 1), (0, 2)) for i in range(2) for slot in slots]
        for at, (slot, i) in enumerate(steps):
            down(slot, i)
            if at:
                settle(*steps[at - 1])
        settle(*steps[-1])
        finish(0, ret_out)
        ret_copy().start()
        finish(1, out_ref)

        ret_copy().wait_send()
        edge_copy().wait_send()
        norm_over(False).wait_send()
        for i in range(2):
            near_copy(i, t).wait_send()
            for c in range(2):
                pair_copy(far_first + c, i).wait_send()
                far_copy(far_first + c, i).wait_send()
        for m, c in pieces:
            hop(m, None, 1, 0, c).wait_send()
            hop(m, 0, 2, 0, c).wait_send()
            for j in range(1, groups):
                if (m, c) in crossed:
                    cross(m, 0, c, j).wait_send()
                cross(m, 1, c, j).wait_send()
                cross(m, 2, c, j).wait_send()

    @pl.when(has_left)
    def _():
        for i in range(2):
            halo_copy(i, True).wait_send()

    @pl.when(has_right)
    def _():
        for i in range(2):
            halo_copy(i, False).wait_send()

    for step in range(3):
        spread(*proj_args, step).wait_send()
        spread(*mix_args, step).wait_send()


def kernel_shards(
    sizes, queries, keys, values, sink, resid, out_proj, norm_gain, w_gate, w_up, conv_w, conv_b, w_down
):
    groups, n, tps = sizes
    tokens, width = resid.shape
    cols = out_proj.shape[1]
    depth, hidden = w_gate.shape
    vmem = pl.BlockSpec(memory_space=pltpu.VMEM)
    dma = pltpu.SemaphoreType.DMA
    cross_sems = dma((3, 3, CHUNKS, groups))
    return pl.pallas_call(
        functools.partial(layer_kernel, sizes),
        out_shape=jax.ShapeDtypeStruct((tokens, cols), BF16),
        in_specs=[vmem] * 3 + [pl.BlockSpec(memory_space=pltpu.SMEM)] + [vmem] * 8,
        out_specs=vmem,
        scratch_shapes=[
            pltpu.VMEM((2, tokens + 2 * WINDOW, HD), BF16),
            pltpu.VMEM((tps,) + out_proj.shape, BF16),
            pltpu.VMEM((tps,) + queries.shape, BF16),
            pltpu.VMEM((tokens // 2, width), F32),
            pltpu.VMEM((2 * tokens, width), BF16),
            pltpu.VMEM((n - 1,) + w_gate.shape, BF16),
            pltpu.VMEM((n - 1,) + w_up.shape, BF16),
            pltpu.VMEM((n - 1,) + w_down.shape, BF16),
            pltpu.VMEM((2 * tokens + 2 * PAD, hidden), F32),
            pltpu.VMEM((2 * tokens, hidden), F32),
            pltpu.VMEM((EDGE, hidden), BF16),
            pltpu.VMEM((EDGE, hidden), BF16),
            pltpu.VMEM((2 * tokens, hidden), BF16),
            pltpu.VMEM((tps, 2 * tokens, cols), BF16),
            pltpu.VMEM((tps, 2 * tokens, cols), BF16),
            pltpu.VMEM((2, 2, tokens // 2, cols), BF16),
            pltpu.VMEM((tokens, cols), BF16),
            pltpu.VMEM((tokens, cols), BF16),
            dma((2, 2)), dma((2, 2)),
            dma((3, 3, groups, CHUNKS)), dma((3, 2, groups, CHUNKS)),
            cross_sems, cross_sems,
            dma((3,)), dma((3,)), dma((3,)), dma((3,)), dma((2,)), dma((2,)), dma((1,)), dma((1,)),
            dma((tps, 2)), dma((tps, 2)), dma((2, 2)), dma((2, 2)), dma((1,)), dma((1,)),
        ],
        compiler_params=pltpu.CompilerParams(
            collective_id=0, has_side_effects=True, vmem_limit_bytes=67043328
        ),
    )(queries, keys, values, sink, resid, out_proj, norm_gain[None], w_gate, w_up, conv_w, conv_b[None], w_down)


def fits_kernel(sizes, args):
    groups, n, tps = sizes
    queries, resid, out_proj, w_gate, w_down = args[0], args[4], args[5], args[7], args[11]
    part = groups * CHUNKS * EDGE
    weights = 3 * 2 * n * w_gate.shape[0] * w_gate.shape[1]
    return (
        n == 4
        and tps == 4
        and groups > 1
        and w_down.shape[1] == out_proj.shape[1]
        and w_gate.shape[0] % max(part, 128) == 0
        and w_down.shape[0] % part == 0
        and w_down.shape[1] % 256 == 0
        and w_gate.shape[1] % out_proj.shape[1] == 0
        and resid.shape[0] % (4 * WINDOW) == 0
        and weights <= 20 * 2 ** 20
    )


def run_shards(sizes, *args):
    if fits_kernel(sizes, args):
        return kernel_shards(sizes, *args)
    return shards(*args)


def solution(mesh):
    sizes = tuple(mesh.shape[axis] for axis in ("grp", "sp", "tp"))
    return jax.shard_map(
        functools.partial(run_shards, sizes),
        mesh=mesh,
        in_specs=(
            P(("grp", "sp"), "tp"),
            P(("grp", "sp"), None),
            P(("grp", "sp"), None),
            P("tp"),
            P(("grp", "sp"), None),
            P(None, "tp"),
            P(),
            P("sp", "tp"),
            P("sp", "tp"),
            P(None, "tp"),
            P("tp"),
            P("tp", "sp"),
        ),
        out_specs=P(("grp", "sp"), "tp"),
        check_vma=False,
    )
```

profile of v0, /device:TPU:16, one launch (start us, length us, event | category | flops | bytes accessed | tf_op | source)
XLA Modules:
  0.0 162.9 jit_solution(1850099578884726359)
XLA Ops:
  0.0 1.3 broadcast_in_dim.7.cb_ref
  1.3 159.7 %shard_map.118 = bf16[512,512]{1,0:T(8,128)(2,1)} custom-call(bf16[512,256]{1,0:T(8,128)(2,1)} %q_ref.1, bf16[512,256]{1,0:T(8,128)(2,1)} %k_ref.1, bf16[512,256]{1,0:T(8,128)(2,1)} %v_ref.1, f32[2]{0:T(128)} %sink_ref.1, bf16[512,2048]{1,0:T(8,128)(2,1)} %resid_ref.1, bf16[1024,512]{1,0:T(8,128)(2,1)} %proj_ref.1, f32[1,2048]{1,0:T(1,128)} %bitcast.1, ...), custom_call_target="tpu_custom_call" | custom-call | tf_op jit(solution)/shard_map/pallas_call | solution.py:582
  161.0 1.9 %copy.14 = bf16[512,512]{1,0:T(8,128)(2,1)} copy(bf16[512,512]{1,0:T(8,128)(2,1)} %shard_map.118) | data formatting | bytes 1048576
where the time goes:
time: 165 us; the launch traced here: 163 us
  Pallas kernels  160 us (97%)
  local copies, waits for them, and re-layouts  3.16 us (2%)
    pallas_call x1, Pallas kernels, kernel_shards(): pl.pallas_call(functools.partial(layer_kernel, sizes), out_shape=jax.Shap...  160 us

commit v1 on v0

v1 whole, which is shorter than its diff:
```python
import functools

import jax
import jax.numpy as jnp
from jax import lax
from jax.experimental import pallas as pl
from jax.experimental.pallas import tpu as pltpu
from jax.sharding import PartitionSpec as P

H = 8
KVH = 2
HD = 128
WINDOW = 128
CONV = 3


def with_halo(cells, sides, width):
    for axis, dim in sides:
        count = lax.axis_size(axis)
        ends = count - 1
        head = lax.slice_in_dim(cells, 0, width, axis=dim)
        tail = lax.slice_in_dim(cells, cells.shape[dim] - width, cells.shape[dim], axis=dim)
        cells = jnp.concatenate(
            [
                lax.ppermute(tail, axis, [(i, (i + 1) % count) for i in range(ends)]),
                cells,
                lax.ppermute(head, axis, [((i + 1) % count, i) for i in range(ends)]),
            ],
            axis=dim,
        )
    return cells


def shards(
    queries, keys, values, sink, resid, out_proj, norm_gain, w_gate, w_up, conv_w, conv_b, w_down
):
    tokens = queries.shape[0]
    width = resid.shape[1]
    heads_here = sink.shape[0]
    group = H // KVH
    scale = HD ** (-0.5)
    first_head = lax.axis_index("tp") * heads_here
    kv_head = first_head // group
    own_keys = lax.dynamic_slice_in_dim(keys, kv_head * HD, HD, 1)
    own_values = lax.dynamic_slice_in_dim(values, kv_head * HD, HD, 1)
    extended = with_halo(jnp.stack([own_keys, own_values]), (("sp", 1),), WINDOW)
    ext_keys = extended[0]
    ext_values = extended[1]
    span = tokens + 2 * WINDOW
    q_heads = queries.reshape(tokens, heads_here, HD)
    scores = (
        jnp.einsum("qhd,kd->hqk", q_heads, ext_keys, preferred_element_type=jnp.float32) * scale
    )
    offset = lax.axis_index("sp") * tokens
    q_pos = offset + jnp.arange(tokens, dtype=jnp.int32)[:, None]
    k_pos = offset - WINDOW + jnp.arange(span, dtype=jnp.int32)[None, :]
    seq_total = tokens * lax.axis_size("sp")
    valid = (jnp.abs(q_pos - k_pos) <= WINDOW) & (k_pos >= 0) & (k_pos < seq_total)
    scores = jnp.where(valid[None], scores, jnp.float32(-1e30))
    sink_col = sink[:, None]
    top = jnp.maximum(jnp.max(scores, axis=-1), sink_col)
    expo = jnp.exp(scores - top[..., None])
    total = jnp.sum(expo, axis=-1) + jnp.exp(sink_col - top)
    weights = (expo / total[..., None]).astype(jnp.bfloat16)
    heads_out = jnp.einsum("hqk,kd->qhd", weights, ext_values, preferred_element_type=jnp.float32)
    heads_out = heads_out.astype(jnp.bfloat16).reshape(tokens, heads_here * HD)
    all_heads = lax.all_gather(heads_out, "tp", axis=1, tiled=True)
    cols = width // lax.axis_size("tp")
    col_start = lax.axis_index("tp") * cols
    full_proj = lax.all_gather(out_proj, "tp", axis=1, tiled=True)
    summed = resid.astype(jnp.float32) + jnp.dot(
        all_heads, full_proj, preferred_element_type=jnp.float32
    )
    mean = jnp.mean(summed, axis=-1, keepdims=True)
    msq = jnp.mean(summed * summed, axis=-1, keepdims=True)
    normed_full = ((summed - mean) * lax.rsqrt(msq - mean * mean + 1e-05) * norm_gain).astype(
        jnp.bfloat16
    )
    normed_own = lax.dynamic_slice_in_dim(normed_full, col_start, cols, 1)
    gate_acc = jnp.dot(
        normed_full,
        lax.all_gather(w_gate, "sp", axis=0, tiled=True),
        preferred_element_type=jnp.float32,
    )
    up_acc = jnp.dot(
        normed_full,
        lax.all_gather(w_up, "sp", axis=0, tiled=True),
        preferred_element_type=jnp.float32,
    )
    gate_pre = gate_acc.astype(jnp.bfloat16)
    up_part = up_acc.astype(jnp.bfloat16)
    padded = with_halo(gate_pre, (("sp", 0),), CONV // 2)
    conv = conv_b
    for tap in range(CONV):
        conv = conv + padded[tap : tap + tokens].astype(jnp.float32) * conv_w[tap]
    act = (jax.nn.silu(conv) * up_part.astype(jnp.float32)).astype(jnp.bfloat16)
    terms = jnp.dot(
        act, lax.all_gather(w_down, "sp", axis=1, tiled=True), preferred_element_type=jnp.float32
    )
    ffn_own = lax.psum_scatter(
        terms.astype(jnp.bfloat16), "tp", scatter_dimension=1, tiled=True
    ).astype(jnp.float32)
    return (normed_own.astype(jnp.float32) + ffn_own).astype(jnp.bfloat16)


EDGE = 16
SPLIT = 2
BF16 = jnp.bfloat16
F32 = jnp.float32


def layer_kernel(
    sizes,
    q_hbm, k_hbm, v_hbm, sink_ref, resid_hbm, proj_hbm, gain_ref, wg_hbm, wu_hbm, cw_ref, cb_ref, wd_hbm,
    out_ref,
    q_ref, kv_ext, resid_ref, proj_all, mixed, summed, normed, wg_all, wu_all, wd_all, gate, up, act,
    terms, near_in, pair_in, far_in, over_in, ret_out, ret_in,
    local_sem, halo_send, halo_recv, z_send, z_recv, y_send, y_recv,
    proj_send, proj_recv, mix_send, mix_recv, norm_send, norm_recv, edge_send, edge_recv, row_send, row_recv,
    near_send, near_recv, pair_send, pair_recv, far_send, far_recv, over_send, over_recv, ret_send, ret_recv,
):
    groups, n, tps = sizes
    g = lax.axis_index("grp")
    s = lax.axis_index("sp")
    t = lax.axis_index("tp")
    tokens, width = resid_hbm.shape
    heads_here = sink_ref.shape[0]
    cols = proj_hbm.shape[1]
    depth = wg_hbm.shape[0]
    hidden = wg_hbm.shape[1]
    part = hidden // 2
    rows2 = 2 * tokens
    has_left, has_right = s > 0, s < n - 1
    inner = has_left & has_right
    outer = jnp.logical_not(inner)
    low = s < n // 2
    mate = s + 1 - 2 * lax.rem(s, 2)
    mirror = n - 1 - s
    beyond = n - 1 - mate
    role = 1 - jnp.where(inner, 1, 0)
    hidden_at = pl.multiple_of(role * part, 128)
    base = pl.multiple_of(EDGE + lax.rem(s, 2) * tokens, EDGE)
    other_base = pl.multiple_of(EDGE + (1 - lax.rem(s, 2)) * tokens, EDGE)
    core = lax.rem(t, 2)
    core_peer = t + 1 - 2 * core
    chip_peer = lax.rem(t + 2, tps)
    own = (wg_hbm, wu_hbm, wd_hbm)
    full = (wg_all, wu_all, wd_all)
    OWN = n - 1

    def remote(src, dst, send, recv, to):
        return pltpu.make_async_remote_copy(
            src_ref=src, dst_ref=dst, send_sem=send, recv_sem=recv,
            device_id=to, device_id_type=pl.DeviceIdType.MESH,
        )

    kv_head = (t * heads_here) // (H // KVH)
    kv_cols = pl.ds(pl.multiple_of(kv_head * HD, HD), HD)

    def local(i):
        src, dst = (
            (q_hbm, q_ref),
            (k_hbm.at[:, kv_cols], kv_ext.at[0, pl.ds(WINDOW, tokens)]),
            (v_hbm.at[:, kv_cols], kv_ext.at[1, pl.ds(WINDOW, tokens)]),
            (proj_hbm, proj_all.at[t]),
            (resid_hbm, resid_ref),
            (wg_hbm.at[:, pl.ds(hidden_at, part)], wg_all.at[OWN]),
            (wu_hbm.at[:, pl.ds(hidden_at, part)], wu_all.at[OWN]),
            (wd_hbm.at[pl.ds(hidden_at, part)], wd_all.at[OWN]),
        )[i]
        return pltpu.make_async_copy(src, dst, local_sem.at[i])

    for i in range(8):
        local(i).start()

    barrier = pltpu.get_barrier_semaphore()

    def greet(to):
        pl.semaphore_signal(barrier, inc=1, device_id=to, device_id_type=pl.DeviceIdType.MESH)

    for j in range(1, n):
        greet({"sp": lax.rem(s + j, n)})
    for j in range(1, groups):
        greet({"grp": lax.rem(g + j, groups)})
    for j in range(1, tps):
        greet({"tp": lax.rem(t + j, tps)})
    for j in range(2):
        greet({"sp": mate, "tp": lax.rem(t - core + 2 + j, tps)})
    pl.semaphore_wait(barrier, n - 1 + groups - 1 + tps - 1 + 2)

    def halo_copy(i, to_left):
        ref = (k_hbm, v_hbm)[i]
        if to_left:
            return remote(ref.at[pl.ds(0, WINDOW), kv_cols], kv_ext.at[i, pl.ds(WINDOW + tokens, WINDOW)],
                          halo_send.at[i, 0], halo_recv.at[i, 0], {"sp": s - 1})
        return remote(ref.at[pl.ds(tokens - WINDOW, WINDOW), kv_cols], kv_ext.at[i, pl.ds(0, WINDOW)],
                      halo_send.at[i, 1], halo_recv.at[i, 1], {"sp": s + 1})

    def chunk_of(m, of, c):
        if m < 2:
            step = depth // (groups * SPLIT)
            return pl.ds(pl.multiple_of((of * SPLIT + c) * step, EDGE), step)
        step = cols // (groups * SPLIT)
        return pl.ds(pl.multiple_of((c * groups + of) * step, 128), step)

    def source(m, r, c):
        if m < 2:
            return own[m].at[chunk_of(m, g, c), pl.ds(r * part, part)]
        return own[m].at[pl.ds(r * part, part), chunk_of(m, g, c)]

    def place(m, slot, of, c):
        if m < 2:
            return full[m].at[slot, chunk_of(m, of, c)]
        return full[m].at[slot, :, chunk_of(m, of, c)]

    IN_ACROSS, IN_BEYOND, IN_MATE, IN_RELAY, OUT_MATE, OUT_MIRROR = range(6)

    def ship(kind, m, c):
        src, slot, to, lane = {
            IN_ACROSS: (None, 1, mirror, 0),
            IN_BEYOND: (None, 1, beyond, 1),
            IN_MATE: (None, 0, mate, 2),
            IN_RELAY: (0, 2, mirror, 3),
            OUT_MATE: (None, 0, mate, 0),
            OUT_MIRROR: (None, 2, mirror, 1),
        }[kind]
        r = 0 if kind in (IN_ACROSS, OUT_MATE) else 1
        src_ref = source(m, r, c) if src is None else place(m, src, g, c)
        return remote(src_ref, place(m, slot, g, c), z_send.at[m, lane, c], z_recv.at[m, slot, c], {"sp": to})

    def ship_all(kind, m):
        for c in range(SPLIT):
            ship(kind, m, c).start()

    def cross(m, slot, c):
        return remote(place(m, slot, g, c), place(m, slot, g, c), y_send.at[m, slot, c], y_recv.at[m, slot, c],
                      {"grp": 1 - g})

    def cross_arrival(m, slot, c):
        return remote(place(m, slot, 1 - g, c), place(m, slot, 1 - g, c), y_send.at[m, slot, c],
                      y_recv.at[m, slot, c], {"grp": 1 - g})

    def take(m, slot, cs=range(SPLIT)):
        for c in cs:
            remote(place(m, slot, g, c), place(m, slot, g, c), z_send.at[m, 0, c], z_recv.at[m, slot, c],
                   {"sp": mate}).wait_recv()
            cross(m, slot, c).start()
            if slot == 0:
                @pl.when(inner)
                def _():
                    ship(IN_RELAY, m, c).start()

    def have(m, slot, cs=range(SPLIT)):
        for c in cs:
            cross_arrival(m, slot, c).wait_recv()

    def spread(src, ref, send, recv, step):
        origin = (t, t, chip_peer)[step]
        return remote(src if step < 2 else ref.at[origin], ref.at[origin], send.at[step], recv.at[step],
                      {"tp": (core_peer, chip_peer, core_peer)[step]})

    def spread_arrival(src, ref, send, recv, step):
        origin = (core_peer, chip_peer, lax.rem(core_peer + 2, tps))[step]
        return remote(src, ref.at[origin], send.at[step], recv.at[step],
                      {"tp": (core_peer, chip_peer, core_peer)[step]})

    proj_args = (proj_hbm, proj_all, proj_send, proj_recv)
    mix_args = (mixed.at[t], mixed, mix_send, mix_recv)

    @pl.when(has_left)
    def _():
        for i in range(2):
            halo_copy(i, True).start()

    @pl.when(has_right)
    def _():
        for i in range(2):
            halo_copy(i, False).start()

    @pl.when(outer)
    def _():
        for m in range(2):
            ship_all(OUT_MATE, m)
            ship_all(OUT_MIRROR, m)

    @pl.when(inner)
    def _():
        for m in range(2):
            ship_all(IN_ACROSS, m)
            ship_all(IN_BEYOND, m)
            ship_all(IN_MATE, m)

    for step in (1, 0):
        spread(*proj_args, step).start()

    @pl.when(jnp.logical_not(has_left))
    def _():
        kv_ext[:, pl.ds(0, WINDOW), :] = jnp.zeros((2, WINDOW, HD), BF16)

    @pl.when(jnp.logical_not(has_right))
    def _():
        kv_ext[:, pl.ds(WINDOW + tokens, WINDOW), :] = jnp.zeros((2, WINDOW, HD), BF16)

    for i in range(3):
        local(i).wait()

    @pl.when(has_right)
    def _():
        for i in range(2):
            halo_copy(i, True).wait_recv()

    @pl.when(has_left)
    def _():
        for i in range(2):
            halo_copy(i, False).wait_recv()

    span = 3 * WINDOW
    seq_total = tokens * n

    @pl.loop(0, tokens // WINDOW)
    def _(b):
        start = pl.multiple_of(b * WINDOW, WINDOW)
        row = lax.broadcasted_iota(jnp.int32, (WINDOW, span), 0)
        col = lax.broadcasted_iota(jnp.int32, (WINDOW, span), 1)
        k_pos = s * tokens + start - WINDOW + col
        valid = (jnp.abs(row + WINDOW - col) <= WINDOW) & (k_pos >= 0) & (k_pos < seq_total)
        kb = kv_ext[0, pl.ds(start, span), :]
        vb = kv_ext[1, pl.ds(start, span), :]
        for h in range(heads_here):
            qb = q_ref[pl.ds(start, WINDOW), h * HD:(h + 1) * HD]
            sc = lax.dot_general(qb, kb, (((1,), (1,)), ((), ())), preferred_element_type=F32) * (HD ** -0.5)
            sc = jnp.where(valid, sc, F32(-1e30))
            sink = sink_ref[h]
            top = jnp.maximum(jnp.max(sc, axis=-1, keepdims=True), sink)
            expo = jnp.exp(sc - top)
            total = jnp.sum(expo, axis=-1, keepdims=True) + jnp.exp(sink - top)
            weights = (expo / total).astype(BF16)
            o = jnp.dot(weights, vb, preferred_element_type=F32)
            mixed[t, pl.ds(start, WINDOW), h * HD:(h + 1) * HD] = o.astype(BF16)

    for step in (1, 0):
        spread(*mix_args, step).start()

    take(0, 0)

    @pl.when(inner)
    def _():
        take(0, 1)

    for args in (proj_args, mix_args):
        spread_arrival(*args, 1).wait_recv()
        spread(*args, 2).start()
    for args in (proj_args, mix_args):
        for step in (0, 2):
            spread_arrival(*args, step).wait_recv()

    @pl.when(inner)
    def _():
        take(1, 0)

    for i in (3, 4):
        local(i).wait()
    lanes = mixed.shape[2]
    block = summed.shape[0]
    strip = 64

    @pl.loop(0, tokens // block)
    def _(b):
        rows = pl.ds(pl.multiple_of(b * block, block), block)

        @pl.loop(0, tps)
        def _(i):
            at = pl.ds(pl.multiple_of(i * cols, 128), cols)
            prod = jnp.dot(mixed[0, rows, :], proj_all[i, pl.ds(0, lanes), :], preferred_element_type=F32)
            for u in range(1, tps):
                prod += jnp.dot(mixed[u, rows, :], proj_all[i, pl.ds(u * lanes, lanes), :],
                                preferred_element_type=F32)
            summed[:, at] = resid_ref[rows, at].astype(F32) + prod

        @pl.loop(0, block // strip)
        def _(i):
            at = pl.multiple_of(i * strip, strip)
            x = summed[pl.ds(at, strip), :]
            mean = jnp.mean(x, axis=-1, keepdims=True)
            msq = jnp.mean(x * x, axis=-1, keepdims=True)
            normed[pl.ds(pl.multiple_of(base + b * block + at, EDGE), strip), :] = (
                (x - mean) * lax.rsqrt(msq - mean * mean + 1e-05) * gain_ref[...]
            ).astype(BF16)

    my_cols = pl.ds(pl.multiple_of(t * cols, 128), cols)

    def norm_part(first, col):
        return normed.at[pl.ds(first, tokens), pl.ds(pl.multiple_of(col * cols, 128), cols)]

    def norm_copy(i, arrival=False):
        first = base if i == 0 and not arrival else other_base
        col = (t, t, t, chip_peer)[i] if not arrival else (t, chip_peer, core_peer, lax.rem(core_peer + 2, tps))[i]
        to = ({"sp": mate}, {"tp": chip_peer}, {"tp": core_peer}, {"tp": core_peer})[i]
        ref = norm_part(first, col)
        return remote(ref, ref, norm_send.at[i], norm_recv.at[i], to)

    edge_from = pl.ds(pl.multiple_of(base + jnp.where(low, tokens - EDGE, 0), EDGE), EDGE)
    edge_over = pl.ds(pl.multiple_of(jnp.where(low, 0, EDGE + rows2), EDGE), EDGE)
    edge_here = pl.ds(pl.multiple_of(jnp.where(low, EDGE + rows2, 0), EDGE), EDGE)

    def edge_copy(i):
        return remote(normed.at[edge_from, my_cols], normed.at[edge_over, my_cols], edge_send.at[i],
                      edge_recv.at[0], {"sp": (mirror, beyond)[i]})

    def edge_arrival():
        ref = normed.at[edge_here, my_cols]
        return remote(ref, ref, edge_send.at[0], edge_recv.at[0], {"sp": mirror})

    def row_copy(j, arrival=False):
        col = lax.rem(t + tps - j, tps) if arrival else t
        ref = normed.at[edge_here, pl.ds(pl.multiple_of(col * cols, 128), cols)]
        return remote(ref, ref, row_send.at[j - 1], row_recv.at[j - 1], {"tp": lax.rem(t + j, tps)})

    tile = 256

    def source_of(slot):
        return (mate, jnp.where(low, n // 2, n // 2 - 1), jnp.where(low, n - 1, 0), s)[slot]

    with_edge = pl.ds(pl.multiple_of(jnp.where(low, EDGE, 0), EDGE), rows2 + EDGE)
    both = pl.ds(EDGE, rows2)

    def gate_up(slot):
        if slot != OWN:
            have(0, slot)
            have(1, slot)
        k = pl.ds(pl.multiple_of(source_of(slot) * depth, 128), depth)

        @pl.loop(0, part // tile)
        def _(i):
            at = pl.ds(pl.multiple_of(i * tile, 128), tile)
            ga = jnp.dot(normed[with_edge, k], wg_all[slot, :, at], preferred_element_type=F32)
            if slot == OWN:
                gate[with_edge, at] = ga
            else:
                gate[with_edge, at] += ga
            ub = jnp.dot(normed[both, k], wu_all[slot, :, at], preferred_element_type=F32)
            if slot == OWN:
                up[:, at] = ub
            else:
                up[:, at] += ub

    @pl.when(inner)
    def _():
        for i in range(2):
            edge_copy(i).start()

    norm_copy(0).start()

    @pl.when(outer)
    def _():
        ship_all(OUT_MATE, 2)
        take(0, 1)
        take(1, 0)

    @pl.when(inner)
    def _():
        ship_all(IN_MATE, 2)
        ship_all(IN_BEYOND, 2)
        ship_all(IN_ACROSS, 2)

    for i in (5, 6, 7):
        local(i).wait()

    take(1, 1)
    norm_copy(0, True).wait_recv()
    norm_copy(1).start()
    norm_copy(2).start()
    take(0, 2)

    @pl.when(inner)
    def _():
        take(2, 0)

    norm_copy(1, True).wait_recv()
    norm_copy(3).start()

    @pl.when(outer)
    def _():
        ship_all(OUT_MIRROR, 2)

    edge_arrival().wait_recv()
    for j in range(1, tps):
        row_copy(j).start()
    norm_copy(2, True).wait_recv()
    norm_copy(3, True).wait_recv()
    for j in range(1, tps):
        row_copy(j, True).wait_recv()
    gate_up(OWN)
    gate_up(0)
    gate_up(1)
    take(1, 2)

    @pl.when(outer)
    def _():
        take(2, 0)

    gate_up(2)

    @pl.when(low)
    def _():
        gate[0:EDGE, :] = jnp.zeros((EDGE, part), F32)

    @pl.when(jnp.logical_not(low))
    def _():
        gate[EDGE + rows2:, :] = jnp.zeros((EDGE, part), F32)

    @pl.loop(0, part // 128)
    def _(i):
        at = pl.ds(pl.multiple_of(i * 128, 128), 128)
        ch = pl.ds(pl.multiple_of(hidden_at + i * 128, 128), 128)
        gate[:, at] = gate[:, at].astype(BF16).astype(F32)
        conv = cb_ref[:, ch]
        for tap in range(CONV):
            conv = conv + gate[pl.ds(EDGE - CONV // 2 + tap, rows2), at] * cw_ref[tap:tap + 1, ch]
        silu = conv / (1.0 + jnp.exp(-conv))
        act[:, at] = (silu * up[:, at].astype(BF16).astype(F32)).astype(BF16)

    half_rows = tokens // 2
    wide = cols // SPLIT
    far_first = (1 - t // 2) * 2

    def is_far(p):
        return (p // 2) != (t // 2)

    def rows_of(i):
        return pl.ds(pl.multiple_of((base if i else other_base) - EDGE, tokens), tokens)

    def half_of(i, c):
        first = (base if i else other_base) - EDGE + c * half_rows
        return pl.ds(pl.multiple_of(first, half_rows), half_rows)

    def half_rows_of(c):
        return pl.ds(pl.multiple_of(c * half_rows, half_rows), half_rows)

    def block_of(c):
        return pl.ds(c * wide, wide)

    def near_copy(i, c):
        return remote(terms.at[core_peer, rows_of(i), block_of(c)], near_in.at[i, :, block_of(c)],
                      near_send.at[i, c], near_recv.at[i, c], {"tp": core_peer})

    def pair_copy(p, i, c):
        q = lax.rem(p, 2)
        return remote(terms.at[p, half_of(i, 1 - core), block_of(c)], pair_in.at[q, i, :, block_of(c)],
                      pair_send.at[q, i, c], pair_recv.at[q, i, c], {"tp": core_peer})

    def far_copy(p, i, c):
        q = lax.rem(p, 2)
        src = terms.at[p, half_of(i, core), block_of(c)]
        if i:
            return remote(src, far_in.at[half_rows_of(core), block_of(c)], far_send.at[q, i, c],
                          far_recv.at[core, c], {"tp": p})
        return remote(src, over_in.at[half_rows_of(core), block_of(c)], far_send.at[q, i, c],
                      over_recv.at[core, c], {"sp": mate, "tp": p})

    def far_arrival(h, c):
        ref = far_in.at[half_rows_of(h), block_of(c)]
        return remote(ref, ref, over_send.at[h, c], far_recv.at[h, c], {"tp": far_first + h})

    def over_arrival(h, c):
        ref = over_in.at[half_rows_of(h), block_of(c)]
        return remote(ref, ref, over_send.at[h, c], over_recv.at[h, c], {"sp": mate, "tp": far_first + h})

    def ret_copy(c):
        return remote(ret_out.at[:, block_of(c)], ret_in.at[:, block_of(c)], ret_send.at[c], ret_recv.at[c],
                      {"sp": mate})

    def down(slot, c, i):
        p = source_of(slot)
        w = wd_all[slot, :, block_of(c)]
        terms[p, rows_of(i), block_of(c)] = jnp.dot(act[rows_of(i), :], w, preferred_element_type=F32).astype(BF16)

        @pl.when(p == core_peer)
        def _():
            near_copy(i, c).start()

        @pl.when(is_far(p))
        def _():
            pair_copy(p, i, c).start()

    def settle(slot, c, i):
        p = source_of(slot)

        @pl.when(is_far(p))
        def _():
            pair_copy(p, i, c).wait_recv()
            rows = half_of(i, core)
            both = (terms[p, rows, block_of(c)].astype(F32)
                    + pair_in[lax.rem(p, 2), i, :, block_of(c)].astype(F32))
            terms[p, rows, block_of(c)] = both.astype(BF16)
            far_copy(p, i, c).start()

        if i == 0:
            @pl.when(p == t)
            def _():
                near_copy(0, c).wait_recv()
                ret_out[:, block_of(c)] = (terms[t, rows_of(0), block_of(c)].astype(F32)
                                           + near_in[0, :, block_of(c)].astype(F32)).astype(BF16)
                ret_copy(c).start()

    def finish(c):
        near_copy(1, c).wait_recv()
        at = pl.ds(pl.multiple_of(t * cols + c * wide, 128), wide)
        out = normed[pl.ds(base, tokens), at].astype(F32) + terms[t, rows_of(1), block_of(c)].astype(F32)
        out = out + near_in[1, :, block_of(c)].astype(F32)
        for h in range(2):
            far_arrival(h, c).wait_recv()
        out = out + far_in[:, block_of(c)].astype(F32)
        ret_copy(c).wait_recv()
        out = out + ret_in[:, block_of(c)].astype(F32)
        for h in range(2):
            over_arrival(h, c).wait_recv()
        out = out + over_in[:, block_of(c)].astype(F32)
        out_ref[:, block_of(c)] = out.astype(BF16)

    def downs(slot, c):
        for i in range(2):
            down(slot, c, i)

    def settles(slot, c):
        for i in range(2):
            settle(slot, c, i)

    early = [(slot, c) for slot in (OWN, 0) for c in range(SPLIT)]
    late = [(slot, c) for slot in (1, 2) for c in range(SPLIT)]
    for at, (slot, c) in enumerate(early):
        if slot != OWN:
            have(2, slot, (c,))
        downs(slot, c)
        if at:
            settles(*early[at - 1])
    take(2, late[0][0], (late[0][1],))
    settles(*early[-1])
    for at, (slot, c) in enumerate(late):
        if at + 1 < len(late):
            take(2, late[at + 1][0], (late[at + 1][1],))
        have(2, slot, (c,))
        downs(slot, c)
        settles(slot, c)
    for c in range(SPLIT):
        finish(c)

    @pl.when(inner)
    def _():
        for kind in (IN_ACROSS, IN_BEYOND, IN_MATE, IN_RELAY):
            for m in range(3):
                for c in range(SPLIT):
                    ship(kind, m, c).wait_send()

    @pl.when(outer)
    def _():
        for kind in (OUT_MATE, OUT_MIRROR):
            for m in range(3):
                for c in range(SPLIT):
                    ship(kind, m, c).wait_send()

    for m in range(3):
        for slot in range(n - 1):
            for c in range(SPLIT):
                cross(m, slot, c).wait_send()
    for i in range(4):
        norm_copy(i).wait_send()
    for j in range(1, tps):
        row_copy(j).wait_send()

    @pl.when(inner)
    def _():
        for i in range(2):
            edge_copy(i).wait_send()

    for c in range(SPLIT):
        ret_copy(c).wait_send()
        for i in range(2):
            near_copy(i, c).wait_send()
            for h in range(2):
                pair_copy(far_first + h, i, c).wait_send()
                far_copy(far_first + h, i, c).wait_send()

    @pl.when(has_left)
    def _():
        for i in range(2):
            halo_copy(i, True).wait_send()

    @pl.when(has_right)
    def _():
        for i in range(2):
            halo_copy(i, False).wait_send()

    for step in range(3):
        spread(*proj_args, step).wait_send()
        spread(*mix_args, step).wait_send()


def kernel_shards(
    sizes, queries, keys, values, sink, resid, out_proj, norm_gain, w_gate, w_up, conv_w, conv_b, w_down
):
    groups, n, tps = sizes
    tokens, width = resid.shape
    cols = out_proj.shape[1]
    depth, hidden = w_gate.shape
    part = hidden // 2
    vmem = pl.BlockSpec(memory_space=pltpu.VMEM)
    hbm = pl.BlockSpec(memory_space=pl.ANY)
    smem = pl.BlockSpec(memory_space=pltpu.SMEM)
    dma = pltpu.SemaphoreType.DMA
    block = (tokens, cols)
    return pl.pallas_call(
        functools.partial(layer_kernel, sizes),
        out_shape=jax.ShapeDtypeStruct((tokens, cols), BF16),
        in_specs=[hbm] * 3 + [smem, hbm, hbm, vmem, hbm, hbm, vmem, vmem, hbm],
        out_specs=vmem,
        scratch_shapes=[
            pltpu.VMEM(queries.shape, BF16),
            pltpu.VMEM((2, tokens + 2 * WINDOW, HD), BF16),
            pltpu.VMEM(resid.shape, BF16),
            pltpu.VMEM((tps,) + out_proj.shape, BF16),
            pltpu.VMEM((tps,) + queries.shape, BF16),
            pltpu.VMEM((tokens // 2, width), F32),
            pltpu.VMEM((2 * tokens + 2 * EDGE, width), BF16),
            pltpu.VMEM((n, depth, part), BF16),
            pltpu.VMEM((n, depth, part), BF16),
            pltpu.VMEM((n, part, cols), BF16),
            pltpu.VMEM((2 * tokens + 2 * EDGE, part), F32),
            pltpu.VMEM((2 * tokens, part), F32),
            pltpu.VMEM((2 * tokens, part), BF16),
            pltpu.VMEM((tps, 2 * tokens, cols), BF16),
            pltpu.VMEM((2,) + block, BF16),
            pltpu.VMEM((2, 2, tokens // 2, cols), BF16),
            pltpu.VMEM(block, BF16),
            pltpu.VMEM(block, BF16),
            pltpu.VMEM(block, BF16),
            pltpu.VMEM(block, BF16),
            dma((8,)), dma((2, 2)), dma((2, 2)),
            dma((3, 4, SPLIT)), dma((3, 3, SPLIT)), dma((3, 3, SPLIT)), dma((3, 3, SPLIT)),
            dma((3,)), dma((3,)), dma((3,)), dma((3,)), dma((4,)), dma((4,)), dma((2,)), dma((1,)),
            dma((3,)), dma((3,)),
            dma((2, SPLIT)), dma((2, SPLIT)), dma((2, 2, SPLIT)), dma((2, 2, SPLIT)),
            dma((2, 2, SPLIT)), dma((2, SPLIT)), dma((2, SPLIT)), dma((2, SPLIT)), dma((SPLIT,)), dma((SPLIT,)),
        ],
        compiler_params=pltpu.CompilerParams(
            collective_id=0, has_side_effects=True, vmem_limit_bytes=67043328
        ),
    )(queries, keys, values, sink, resid, out_proj, norm_gain[None], w_gate, w_up, conv_w, conv_b[None], w_down)


def fits_kernel(sizes, args):
    groups, n, tps = sizes
    queries, resid, out_proj, w_gate, w_down = args[0], args[4], args[5], args[7], args[11]
    share = groups * SPLIT
    weights = 3 * 2 * n * w_gate.shape[0] * w_gate.shape[1]
    return (
        n == 4
        and tps == 4
        and groups == 2
        and w_down.shape[1] == out_proj.shape[1]
        and w_gate.shape[0] % max(share * EDGE, 128) == 0
        and w_down.shape[1] % (share * 128) == 0
        and w_gate.shape[1] % 512 == 0
        and resid.shape[0] % (4 * WINDOW) == 0
        and weights <= 20 * 2 ** 20
    )


def run_shards(sizes, *args):
    if fits_kernel(sizes, args):
        return kernel_shards(sizes, *args)
    return shards(*args)


def solution(mesh):
    sizes = tuple(mesh.shape[axis] for axis in ("grp", "sp", "tp"))
    return jax.shard_map(
        functools.partial(run_shards, sizes),
        mesh=mesh,
        in_specs=(
            P(("grp", "sp"), "tp"),
            P(("grp", "sp"), None),
            P(("grp", "sp"), None),
            P("tp"),
            P(("grp", "sp"), None),
            P(None, "tp"),
            P(),
            P("sp", "tp"),
            P("sp", "tp"),
            P(None, "tp"),
            P("tp"),
            P("tp", "sp"),
        ),
        out_specs=P(("grp", "sp"), "tp"),
        check_vma=False,
    )
```

time: 165 us -> 147 us (0.89); the launches traced: 163 us -> 147 us
  Pallas kernels: 160 us -> 144 us
    pallas_call x1, Pallas kernels: 160 us -> 144 us  [kernel_shards(): pl.pallas_call(functools.partial(layer_kernel, sizes), out_shape=jax.Shap...]
where the time goes in v1:
time: 147 us
  Pallas kernels  144 us (98%)
  local copies, waits for them, and re-layouts  3.16 us (2%)
    pallas_call x1, Pallas kernels, kernel_shards(): pl.pallas_call(functools.partial(layer_kernel, sizes), out_shape=jax.Shap...  144 us

profile of v1, /device:TPU:16, one launch (start us, length us, event | category | flops | bytes accessed | tf_op | source)
XLA Modules:
  0.0 146.8 jit_solution(10013204663710712589)
XLA Ops:
  0.0 1.3 broadcast_in_dim.7.cb_ref
  1.3 143.6 %shard_map.118 = bf16[512,512]{1,0:T(8,128)(2,1)} custom-call(bf16[512,256]{1,0:T(8,128)(2,1)} %q_hbm.1, bf16[512,256]{1,0:T(8,128)(2,1)} %k_hbm.1, bf16[512,256]{1,0:T(8,128)(2,1)} %v_hbm.1, f32[2]{0:T(128)} %sink_ref.1, bf16[512,2048]{1,0:T(8,128)(2,1)} %resid_hbm.1, bf16[1024,512]{1,0:T(8,128)(2,1)} %proj_hbm.1, f32[1,2048]{1,0:T(1,128)} %bitcast.1, ...), custom_call_target="tpu_custom_call" | custom-call | tf_op jit(solution)/shard_map/pallas_call | solution.py:712
  144.9 1.9 %copy.14 = bf16[512,512]{1,0:T(8,128)(2,1)} copy(bf16[512,512]{1,0:T(8,128)(2,1)} %shard_map.118) | data formatting | bytes 1048576

commit v2 on v1

--- a/solution.py
+++ b/solution.py
@@ -109,15 +109,19 @@
 F32 = jnp.float32
 
 
+def parts_of(hidden):
+    return hidden * 2 // 3, hidden // 3
+
+
 def layer_kernel(
     sizes,
     q_hbm, k_hbm, v_hbm, sink_ref, resid_hbm, proj_hbm, gain_ref, wg_hbm, wu_hbm, cw_ref, cb_ref, wd_hbm,
     out_ref,
     q_ref, kv_ext, resid_ref, proj_all, mixed, summed, normed, wg_all, wu_all, wd_all, gate, up, act,
-    terms, near_in, pair_in, far_in, over_in, ret_out, ret_in,
+    terms, near_in, pair_in, far_in, mid_in, ret_out, ret_in,
     local_sem, halo_send, halo_recv, z_send, z_recv, y_send, y_recv,
     proj_send, proj_recv, mix_send, mix_recv, norm_send, norm_recv, edge_send, edge_recv, row_send, row_recv,
-    near_send, near_recv, pair_send, pair_recv, far_send, far_recv, over_send, over_recv, ret_send, ret_recv,
+    near_send, near_recv, pair_send, pair_recv, far_send, far_recv, mid_send, mid_recv, ret_send, ret_recv,
 ):
     groups, n, tps = sizes
     g = lax.axis_index("grp")
@@ -128,7 +132,8 @@
     cols = proj_hbm.shape[1]
     depth = wg_hbm.shape[0]
     hidden = wg_hbm.shape[1]
-    part = hidden // 2
+    parts = parts_of(hidden)
+    starts = (0, parts[0])
     rows2 = 2 * tokens
     has_left, has_right = s > 0, s < n - 1
     inner = has_left & has_right
@@ -138,7 +143,8 @@
     mirror = n - 1 - s
     beyond = n - 1 - mate
     role = 1 - jnp.where(inner, 1, 0)
-    hidden_at = pl.multiple_of(role * part, 128)
+    hidden_at = pl.multiple_of(role * parts[0], 128)
+    my_part = jnp.where(inner, parts[0], parts[1])
     base = pl.multiple_of(EDGE + lax.rem(s, 2) * tokens, EDGE)
     other_base = pl.multiple_of(EDGE + (1 - lax.rem(s, 2)) * tokens, EDGE)
     core = lax.rem(t, 2)
@@ -157,21 +163,29 @@
     kv_head = (t * heads_here) // (H // KVH)
     kv_cols = pl.ds(pl.multiple_of(kv_head * HD, HD), HD)
 
-    def local(i):
+    def by_role(fn):
+        for r, here in enumerate((inner, outer)):
+            @pl.when(here)
+            def _():
+                fn(r)
+
+    def local(i, r=0):
+        here, mine = pl.ds(starts[r], parts[r]), pl.ds(0, parts[r])
         src, dst = (
             (q_hbm, q_ref),
             (k_hbm.at[:, kv_cols], kv_ext.at[0, pl.ds(WINDOW, tokens)]),
             (v_hbm.at[:, kv_cols], kv_ext.at[1, pl.ds(WINDOW, tokens)]),
             (proj_hbm, proj_all.at[t]),
             (resid_hbm, resid_ref),
-            (wg_hbm.at[:, pl.ds(hidden_at, part)], wg_all.at[OWN]),
-            (wu_hbm.at[:, pl.ds(hidden_at, part)], wu_all.at[OWN]),
-            (wd_hbm.at[pl.ds(hidden_at, part)], wd_all.at[OWN]),
+            (wg_hbm.at[:, here], wg_all.at[OWN, :, mine]),
+            (wu_hbm.at[:, here], wu_all.at[OWN, :, mine]),
+            (wd_hbm.at[here], wd_all.at[OWN, mine]),
         )[i]
         return pltpu.make_async_copy(src, dst, local_sem.at[i])
 
-    for i in range(8):
+    for i in range(5):
         local(i).start()
+    by_role(lambda r: [local(i, r).start() for i in (5, 6, 7)])
 
     barrier = pltpu.get_barrier_semaphore()
 
@@ -184,9 +198,7 @@
         greet({"grp": lax.rem(g + j, groups)})
     for j in range(1, tps):
         greet({"tp": lax.rem(t + j, tps)})
-    for j in range(2):
-        greet({"sp": mate, "tp": lax.rem(t - core + 2 + j, tps)})
-    pl.semaphore_wait(barrier, n - 1 + groups - 1 + tps - 1 + 2)
+    pl.semaphore_wait(barrier, n - 1 + groups - 1 + tps - 1)
 
     def halo_copy(i, to_left):
         ref = (k_hbm, v_hbm)[i]
@@ -203,56 +215,64 @@
         step = cols // (groups * SPLIT)
         return pl.ds(pl.multiple_of((c * groups + of) * step, 128), step)
 
-    def source(m, r, c):
+    def source(m, r, of, c):
         if m < 2:
-            return own[m].at[chunk_of(m, g, c), pl.ds(r * part, part)]
-        return own[m].at[pl.ds(r * part, part), chunk_of(m, g, c)]
-
-    def place(m, slot, of, c):
+            return own[m].at[chunk_of(m, of, c), pl.ds(starts[r], parts[r])]
+        return own[m].at[pl.ds(starts[r], parts[r]), chunk_of(m, of, c)]
+
+    def place(m, slot, r, of, c):
         if m < 2:
-            return full[m].at[slot, chunk_of(m, of, c)]
-        return full[m].at[slot, :, chunk_of(m, of, c)]
-
-    IN_ACROSS, IN_BEYOND, IN_MATE, IN_RELAY, OUT_MATE, OUT_MIRROR = range(6)
+            return full[m].at[slot, chunk_of(m, of, c), pl.ds(0, parts[r])]
+        return full[m].at[slot, pl.ds(0, parts[r]), chunk_of(m, of, c)]
+
+    IN_ACROSS, IN_BEYOND, IN_MATE, IN_RELAY, OUT_MATE, OUT_MIRROR, OUT_REST = range(7)
 
     def ship(kind, m, c):
-        src, slot, to, lane = {
-            IN_ACROSS: (None, 1, mirror, 0),
-            IN_BEYOND: (None, 1, beyond, 1),
-            IN_MATE: (None, 0, mate, 2),
-            IN_RELAY: (0, 2, mirror, 3),
-            OUT_MATE: (None, 0, mate, 0),
-            OUT_MIRROR: (None, 2, mirror, 1),
+        slot, to, lane = {
+            IN_ACROSS: (1, mirror, 0),
+            IN_BEYOND: (1, beyond, 1),
+            IN_MATE: (0, mate, 2),
+            IN_RELAY: (2, mirror, 3),
+            OUT_MATE: (0, mate, 0),
+            OUT_MIRROR: (2, mirror, 1),
+            OUT_REST: (0, mate, 2),
         }[kind]
-        r = 0 if kind in (IN_ACROSS, OUT_MATE) else 1
-        src_ref = source(m, r, c) if src is None else place(m, src, g, c)
-        return remote(src_ref, place(m, slot, g, c), z_send.at[m, lane, c], z_recv.at[m, slot, c], {"sp": to})
+        r = 0 if kind in (IN_ACROSS, IN_RELAY, OUT_MATE, OUT_REST) else 1
+        of = 1 - g if kind == OUT_REST else g
+        src = place(m, 0, r, of, c) if kind == IN_RELAY else source(m, r, of, c)
+        arrive = y_recv.at[m, slot, c] if kind == OUT_REST else z_recv.at[m, slot, c]
+        return remote(src, place(m, slot, r, of, c), z_send.at[m, lane, c], arrive, {"sp": to})
 
     def ship_all(kind, m):
         for c in range(SPLIT):
             ship(kind, m, c).start()
 
-    def cross(m, slot, c):
-        return remote(place(m, slot, g, c), place(m, slot, g, c), y_send.at[m, slot, c], y_recv.at[m, slot, c],
+    def direct(m, slot, r):
+        return r == 0 and m == 2 and isinstance(slot, int) and slot == 0
+
+    def cross(m, slot, r, c):
+        return remote(place(m, slot, r, g, c), place(m, slot, r, g, c), y_send.at[m, slot, c], y_recv.at[m, slot, c],
                       {"grp": 1 - g})
 
-    def cross_arrival(m, slot, c):
-        return remote(place(m, slot, 1 - g, c), place(m, slot, 1 - g, c), y_send.at[m, slot, c],
-                      y_recv.at[m, slot, c], {"grp": 1 - g})
-
     def take(m, slot, cs=range(SPLIT)):
-        for c in cs:
-            remote(place(m, slot, g, c), place(m, slot, g, c), z_send.at[m, 0, c], z_recv.at[m, slot, c],
-                   {"sp": mate}).wait_recv()
-            cross(m, slot, c).start()
-            if slot == 0:
-                @pl.when(inner)
-                def _():
+        def run(r):
+            for c in cs:
+                remote(place(m, slot, r, g, c), place(m, slot, r, g, c), z_send.at[m, 0, c], z_recv.at[m, slot, c],
+                       {"sp": mate}).wait_recv()
+                if not direct(m, slot, r):
+                    cross(m, slot, r, c).start()
+                if isinstance(slot, int) and slot == 0 and r == 0:
                     ship(IN_RELAY, m, c).start()
 
+        by_role(run)
+
     def have(m, slot, cs=range(SPLIT)):
-        for c in cs:
-            cross_arrival(m, slot, c).wait_recv()
+        def run(r):
+            for c in cs:
+                ref = place(m, slot, r, 1 - g, c)
+                remote(ref, ref, y_send.at[m, slot, c], y_recv.at[m, slot, c], {"grp": 1 - g}).wait_recv()
+
+        by_role(run)
 
     def spread(src, ref, send, recv, step):
         origin = (t, t, chip_peer)[step]
@@ -279,16 +299,16 @@
 
     @pl.when(outer)
     def _():
-        for m in range(2):
-            ship_all(OUT_MATE, m)
-            ship_all(OUT_MIRROR, m)
-
-    @pl.when(inner)
-    def _():
-        for m in range(2):
-            ship_all(IN_ACROSS, m)
-            ship_all(IN_BEYOND, m)
-            ship_all(IN_MATE, m)
+        ship_all(OUT_MATE, 0)
+        ship_all(OUT_MATE, 1)
+        ship_all(OUT_MIRROR, 0)
+
+    @pl.when(inner)
+    def _():
+        ship_all(IN_ACROSS, 0)
+        ship_all(IN_BEYOND, 0)
+        ship_all(IN_MATE, 0)
+        ship_all(IN_MATE, 1)
 
     for step in (1, 0):
         spread(*proj_args, step).start()
@@ -430,7 +450,7 @@
             have(1, slot)
         k = pl.ds(pl.multiple_of(source_of(slot) * depth, 128), depth)
 
-        @pl.loop(0, part // tile)
+        @pl.loop(0, my_part // tile)
         def _(i):
             at = pl.ds(pl.multiple_of(i * tile, 128), tile)
             ga = jnp.dot(normed[with_edge, k], wg_all[slot, :, at], preferred_element_type=F32)
@@ -453,63 +473,80 @@
 
     @pl.when(outer)
     def _():
+        ship_all(OUT_MIRROR, 1)
         ship_all(OUT_MATE, 2)
+        ship_all(OUT_REST, 2)
         take(0, 1)
         take(1, 0)
 
     @pl.when(inner)
     def _():
+        ship_all(IN_ACROSS, 1)
+        ship_all(IN_BEYOND, 1)
         ship_all(IN_MATE, 2)
+        ship_all(IN_ACROSS, 2)
         ship_all(IN_BEYOND, 2)
-        ship_all(IN_ACROSS, 2)
-
-    for i in (5, 6, 7):
-        local(i).wait()
-
-    take(1, 1)
+
+    by_role(lambda r: [local(i, r).wait() for i in (5, 6, 7)])
+
+    take(0, 2)
+
+    @pl.when(inner)
+    def _():
+        take(1, 2)
+
     norm_copy(0, True).wait_recv()
     norm_copy(1).start()
     norm_copy(2).start()
-    take(0, 2)
-
-    @pl.when(inner)
-    def _():
-        take(2, 0)
-
-    norm_copy(1, True).wait_recv()
-    norm_copy(3).start()
-
-    @pl.when(outer)
-    def _():
-        ship_all(OUT_MIRROR, 2)
-
     edge_arrival().wait_recv()
     for j in range(1, tps):
         row_copy(j).start()
+
+    @pl.when(inner)
+    def _():
+        take(1, 1)
+
+    norm_copy(1, True).wait_recv()
+    norm_copy(3).start()
+
+    @pl.when(outer)
+    def _():
+        take(1, 2)
+
     norm_copy(2, True).wait_recv()
     norm_copy(3, True).wait_recv()
     for j in range(1, tps):
         row_copy(j, True).wait_recv()
     gate_up(OWN)
     gate_up(0)
+
+    @pl.when(outer)
+    def _():
+        take(1, 1)
+
+    gate_up(2)
+
+    take(2, 0)
+
     gate_up(1)
-    take(1, 2)
+
+    @pl.when(low)
+    def _():
+        gate[0:EDGE, :] = jnp.zeros((EDGE, parts[0]), F32)
+
+    @pl.when(jnp.logical_not(low))
+    def _():
+        gate[EDGE + rows2:, :] = jnp.zeros((EDGE, parts[0]), F32)
 
     @pl.when(outer)
     def _():
-        take(2, 0)
-
-    gate_up(2)
-
-    @pl.when(low)
-    def _():
-        gate[0:EDGE, :] = jnp.zeros((EDGE, part), F32)
-
-    @pl.when(jnp.logical_not(low))
-    def _():
-        gate[EDGE + rows2:, :] = jnp.zeros((EDGE, part), F32)
-
-    @pl.loop(0, part // 128)
+        ship_all(OUT_MIRROR, 2)
+
+    @pl.when(inner)
+    def _():
+        take(2, 1, (0,))
+
+    @pl.loop(0, my_part // 128)
     def _(i):
         at = pl.ds(pl.multiple_of(i * 128, 128), 128)
         ch = pl.ds(pl.multiple_of(hidden_at + i * 128, 128), 128)
@@ -549,31 +586,30 @@
         return remote(terms.at[p, half_of(i, 1 - core), block_of(c)], pair_in.at[q, i, :, block_of(c)],
                       pair_send.at[q, i, c], pair_recv.at[q, i, c], {"tp": core_peer})
 
-    def far_copy(p, i, c):
+    def mid_copy(p, c):
         q = lax.rem(p, 2)
-        src = terms.at[p, half_of(i, core), block_of(c)]
-        if i:
-            return remote(src, far_in.at[half_rows_of(core), block_of(c)], far_send.at[q, i, c],
-                          far_recv.at[core, c], {"tp": p})
-        return remote(src, over_in.at[half_rows_of(core), block_of(c)], far_send.at[q, i, c],
-                      over_recv.at[core, c], {"sp": mate, "tp": p})
+        return remote(terms.at[p, half_of(0, core), block_of(c)], mid_in.at[q, :, block_of(c)],
+                      mid_send.at[q, c], mid_recv.at[q, c], {"sp": mate})
+
+    def far_copy(p, c):
+        return remote(terms.at[p, half_of(1, core), block_of(c)], far_in.at[half_rows_of(core), block_of(c)],
+                      far_send.at[lax.rem(p, 2), c], far_recv.at[core, c], {"tp": p})
 
     def far_arrival(h, c):
         ref = far_in.at[half_rows_of(h), block_of(c)]
-        return remote(ref, ref, over_send.at[h, c], far_recv.at[h, c], {"tp": far_first + h})
-
-    def over_arrival(h, c):
-        ref = over_in.at[half_rows_of(h), block_of(c)]
-        return remote(ref, ref, over_send.at[h, c], over_recv.at[h, c], {"sp": mate, "tp": far_first + h})
+        return remote(ref, ref, far_send.at[h, c], far_recv.at[h, c], {"tp": far_first + h})
 
     def ret_copy(c):
         return remote(ret_out.at[:, block_of(c)], ret_in.at[:, block_of(c)], ret_send.at[c], ret_recv.at[c],
                       {"sp": mate})
 
-    def down(slot, c, i):
-        p = source_of(slot)
-        w = wd_all[slot, :, block_of(c)]
-        terms[p, rows_of(i), block_of(c)] = jnp.dot(act[rows_of(i), :], w, preferred_element_type=F32).astype(BF16)
+    def down(slot, p, c, i):
+        def run(r):
+            w = wd_all[slot, 0:parts[r], block_of(c)]
+            x = act[rows_of(i), 0:parts[r]]
+            terms[p, rows_of(i), block_of(c)] = jnp.dot(x, w, preferred_element_type=F32).astype(BF16)
+
+        by_role(run)
 
         @pl.when(p == core_peer)
         def _():
@@ -583,25 +619,33 @@
         def _():
             pair_copy(p, i, c).start()
 
-    def settle(slot, c, i):
-        p = source_of(slot)
-
+    def gather(p, c):
+        for i in range(2):
+            @pl.when(is_far(p))
+            def _():
+                pair_copy(p, i, c).wait_recv()
+                rows = half_of(i, core)
+                total = (terms[p, rows, block_of(c)].astype(F32)
+                         + pair_in[lax.rem(p, 2), i, :, block_of(c)].astype(F32))
+                terms[p, rows, block_of(c)] = total.astype(BF16)
+                if i == 0:
+                    mid_copy(p, c).start()
+
+        @pl.when(p == t)
+        def _():
+            near_copy(0, c).wait_recv()
+            ret_out[:, block_of(c)] = (terms[t, rows_of(0), block_of(c)].astype(F32)
+                                       + near_in[0, :, block_of(c)].astype(F32)).astype(BF16)
+            ret_copy(c).start()
+
+    def send_far(p, c):
         @pl.when(is_far(p))
         def _():
-            pair_copy(p, i, c).wait_recv()
-            rows = half_of(i, core)
-            both = (terms[p, rows, block_of(c)].astype(F32)
-                    + pair_in[lax.rem(p, 2), i, :, block_of(c)].astype(F32))
-            terms[p, rows, block_of(c)] = both.astype(BF16)
-            far_copy(p, i, c).start()
-
-        if i == 0:
-            @pl.when(p == t)
-            def _():
-                near_copy(0, c).wait_recv()
-                ret_out[:, block_of(c)] = (terms[t, rows_of(0), block_of(c)].astype(F32)
-                                           + near_in[0, :, block_of(c)].astype(F32)).astype(BF16)
-                ret_copy(c).start()
+            mid_copy(p, c).wait_recv()
+            rows = half_of(1, core)
+            total = terms[p, rows, block_of(c)].astype(F32) + mid_in[lax.rem(p, 2), :, block_of(c)].astype(F32)
+            terms[p, rows, block_of(c)] = total.astype(BF16)
+            far_copy(p, c).start()
 
     def finish(c):
         near_copy(1, c).wait_recv()
@@ -613,35 +657,39 @@
         out = out + far_in[:, block_of(c)].astype(F32)
         ret_copy(c).wait_recv()
         out = out + ret_in[:, block_of(c)].astype(F32)
-        for h in range(2):
-            over_arrival(h, c).wait_recv()
-        out = out + over_in[:, block_of(c)].astype(F32)
         out_ref[:, block_of(c)] = out.astype(BF16)
 
-    def downs(slot, c):
-        for i in range(2):
-            down(slot, c, i)
-
-    def settles(slot, c):
-        for i in range(2):
-            settle(slot, c, i)
-
-    early = [(slot, c) for slot in (OWN, 0) for c in range(SPLIT)]
-    late = [(slot, c) for slot in (1, 2) for c in range(SPLIT)]
-    for at, (slot, c) in enumerate(early):
-        if slot != OWN:
+    def downs(slot, p, c):
+        for i in range(2):
+            down(slot, p, c, i)
+
+    have(2, 0)
+    early = [(jnp.where(inner, OWN, 0), jnp.where(inner, s, mate)), (jnp.where(inner, 0, OWN), jnp.where(inner, mate, s))]
+    early = [(slot, p, c) for slot, p in early for c in range(SPLIT)]
+    late = [(slot, source_of(slot), c) for slot in (1, 2) for c in range(SPLIT)]
+    steps = early + late
+    head = len(early)
+    for at, (slot, p, c) in enumerate(steps):
+        if at == head:
+            gather(*steps[at - 1][1:])
+
+            @pl.when(outer)
+            def _():
+                take(2, slot, (c,))
+
+        if at >= head and at + 1 < len(steps):
+            take(2, steps[at + 1][0], (steps[at + 1][2],))
+        if at >= head:
             have(2, slot, (c,))
-        downs(slot, c)
-        if at:
-            settles(*early[at - 1])
-    take(2, late[0][0], (late[0][1],))
-    settles(*early[-1])
-    for at, (slot, c) in enumerate(late):
-        if at + 1 < len(late):
-            take(2, late[at + 1][0], (late[at + 1][1],))
-        have(2, slot, (c,))
-        downs(slot, c)
-        settles(slot, c)
+        downs(slot, p, c)
+        if at >= head:
+            gather(p, c)
+            send_far(*steps[at - head][1:])
+            if at > head:
+                send_far(*steps[at - 1][1:])
+        elif at:
+            gather(*steps[at - 1][1:])
+    send_far(*steps[-1][1:])
     for c in range(SPLIT):
         finish(c)
 
@@ -654,15 +702,19 @@
 
     @pl.when(outer)
     def _():
-        for kind in (OUT_MATE, OUT_MIRROR):
-            for m in range(3):
+        for kind in (OUT_MATE, OUT_MIRROR, OUT_REST):
+            for m in range(3) if kind != OUT_REST else (2,):
                 for c in range(SPLIT):
                     ship(kind, m, c).wait_send()
 
-    for m in range(3):
-        for slot in range(n - 1):
-            for c in range(SPLIT):
-                cross(m, slot, c).wait_send()
+    def crossed(r):
+        for m in range(3):
+            for slot in range(n - 1):
+                for c in range(SPLIT):
+                    if not direct(m, slot, r):
+                        cross(m, slot, r, c).wait_send()
+
+    by_role(crossed)
     for i in range(4):
         norm_copy(i).wait_send()
     for j in range(1, tps):
@@ -679,7 +731,9 @@
             near_copy(i, c).wait_send()
             for h in range(2):
                 pair_copy(far_first + h, i, c).wait_send()
-                far_copy(far_first + h, i, c).wait_send()
+        for h in range(2):
+            mid_copy(far_first + h, c).wait_send()
+            far_copy(far_first + h, c).wait_send()
 
     @pl.when(has_left)
     def _():
@@ -703,7 +757,7 @@
     tokens, width = resid.shape
     cols = out_proj.shape[1]
     depth, hidden = w_gate.shape
-    part = hidden // 2
+    part = parts_of(hidden)[0]
     vmem = pl.BlockSpec(memory_space=pltpu.VMEM)
     hbm = pl.BlockSpec(memory_space=pl.ANY)
     smem = pl.BlockSpec(memory_space=pltpu.SMEM)
@@ -732,7 +786,7 @@
             pltpu.VMEM((2,) + block, BF16),
             pltpu.VMEM((2, 2, tokens // 2, cols), BF16),
             pltpu.VMEM(block, BF16),
-            pltpu.VMEM(block, BF16),
+            pltpu.VMEM((2, tokens // 2, cols), BF16),
             pltpu.VMEM(block, BF16),
             pltpu.VMEM(block, BF16),
             dma((8,)), dma((2, 2)), dma((2, 2)),
@@ -740,7 +794,7 @@
             dma((3,)), dma((3,)), dma((3,)), dma((3,)), dma((4,)), dma((4,)), dma((2,)), dma((1,)),
             dma((3,)), dma((3,)),
             dma((2, SPLIT)), dma((2, SPLIT)), dma((2, 2, SPLIT)), dma((2, 2, SPLIT)),
-            dma((2, 2, SPLIT)), dma((2, SPLIT)), dma((2, SPLIT)), dma((2, SPLIT)), dma((SPLIT,)), dma((SPLIT,)),
+            dma((2, SPLIT)), dma((2, SPLIT)), dma((2, SPLIT)), dma((2, SPLIT)), dma((SPLIT,)), dma((SPLIT,)),
         ],
         compiler_params=pltpu.CompilerParams(
             collective_id=0, has_side_effects=True, vmem_limit_bytes=67043328
@@ -760,7 +814,7 @@
         and w_down.shape[1] == out_proj.shape[1]
         and w_gate.shape[0] % max(share * EDGE, 128) == 0
         and w_down.shape[1] % (share * 128) == 0
-        and w_gate.shape[1] % 512 == 0
+        and w_gate.shape[1] % 768 == 0
         and resid.shape[0] % (4 * WINDOW) == 0
         and weights <= 20 * 2 ** 20
     )

time: 147 us -> 134 us (0.912)
  Pallas kernels: 144 us -> 131 us
    pallas_call x1, Pallas kernels: 144 us -> 131 us  [kernel_shards(): pl.pallas_call(functools.partial(layer_kernel, sizes), out_shape=jax.Shap...]
where the time goes in v2:
time: 134 us
  Pallas kernels  131 us (98%)
  local copies, waits for them, and re-layouts  3.16 us (2%)
    pallas_call x1, Pallas kernels, kernel_shards(): pl.pallas_call(functools.partial(layer_kernel, sizes), out_shape=jax.Shap...  131 us

profile of v2, /device:TPU:16, one launch (start us, length us, event | category | flops | bytes accessed | tf_op | source)
XLA Modules:
  0.0 133.7 jit_solution(8405360854142074583)
XLA Ops:
  0.0 1.3 broadcast_in_dim.7.cb_ref
  1.3 130.5 %shard_map.118 = bf16[512,512]{1,0:T(8,128)(2,1)} custom-call(bf16[512,256]{1,0:T(8,128)(2,1)} %q_hbm.1, bf16[512,256]{1,0:T(8,128)(2,1)} %k_hbm.1, bf16[512,256]{1,0:T(8,128)(2,1)} %v_hbm.1, f32[2]{0:T(128)} %sink_ref.1, bf16[512,2048]{1,0:T(8,128)(2,1)} %resid_hbm.1, bf16[1024,512]{1,0:T(8,128)(2,1)} %proj_hbm.1, f32[1,2048]{1,0:T(1,128)} %bitcast.1, ...), custom_call_target="tpu_custom_call" | custom-call | tf_op jit(solution)/shard_map/pallas_call | solution.py:766
  131.8 1.9 %copy.14 = bf16[512,512]{1,0:T(8,128)(2,1)} copy(bf16[512,512]{1,0:T(8,128)(2,1)} %shard_map.118) | data formatting | bytes 1048576

commit v3 on v2

--- a/solution.py
+++ b/solution.py
@@ -105,6 +105,7 @@
 
 EDGE = 16
 SPLIT = 2
+PIECES = 4
 BF16 = jnp.bfloat16
 F32 = jnp.float32
 
@@ -117,11 +118,11 @@
     sizes,
     q_hbm, k_hbm, v_hbm, sink_ref, resid_hbm, proj_hbm, gain_ref, wg_hbm, wu_hbm, cw_ref, cb_ref, wd_hbm,
     out_ref,
-    q_ref, kv_ext, resid_ref, proj_all, mixed, summed, normed, wg_all, wu_all, wd_all, gate, up, act,
-    terms, near_in, pair_in, far_in, mid_in, ret_out, ret_in,
+    q_ref, kv_ext, resid_ref, proj_all, mixed, summed, normed, wg_all, wu_all, wd_all, gate, up, silu, act,
+    terms, near_in, pair_in, far_in, mid_in, over_in, ret_out, ret_in,
     local_sem, halo_send, halo_recv, z_send, z_recv, y_send, y_recv,
     proj_send, proj_recv, mix_send, mix_recv, norm_send, norm_recv, edge_send, edge_recv, row_send, row_recv,
-    near_send, near_recv, pair_send, pair_recv, far_send, far_recv, mid_send, mid_recv, ret_send, ret_recv,
+    near_send, near_recv, pair_send, pair_recv, far_send, far_recv, mid_send, mid_recv, over_send, over_recv, ret_send, ret_recv,
 ):
     groups, n, tps = sizes
     g = lax.axis_index("grp")
@@ -198,7 +199,9 @@
         greet({"grp": lax.rem(g + j, groups)})
     for j in range(1, tps):
         greet({"tp": lax.rem(t + j, tps)})
-    pl.semaphore_wait(barrier, n - 1 + groups - 1 + tps - 1)
+    for j in range(2):
+        greet({"sp": mate, "tp": lax.rem(t - core + 2 + j, tps)})
+    pl.semaphore_wait(barrier, n - 1 + groups - 1 + tps - 1 + 2)
 
     def halo_copy(i, to_left):
         ref = (k_hbm, v_hbm)[i]
@@ -208,22 +211,21 @@
         return remote(ref.at[pl.ds(tokens - WINDOW, WINDOW), kv_cols], kv_ext.at[i, pl.ds(0, WINDOW)],
                       halo_send.at[i, 1], halo_recv.at[i, 1], {"sp": s + 1})
 
-    def chunk_of(m, of, c):
+    deep = PIECES // SPLIT
+
+    def window(m, of, c, first, count):
         if m < 2:
-            step = depth // (groups * SPLIT)
-            return pl.ds(pl.multiple_of((of * SPLIT + c) * step, EDGE), step)
+            step = depth // (groups * PIECES)
+            return pl.ds(pl.multiple_of((of * PIECES + c) * step, EDGE), step), pl.ds(first, count)
         step = cols // (groups * SPLIT)
-        return pl.ds(pl.multiple_of((c * groups + of) * step, 128), step)
+        at = pl.multiple_of(((c // deep) * groups + of) * step, 128)
+        return pl.ds(first + (c % deep) * (count // deep), count // deep), pl.ds(at, step)
 
     def source(m, r, of, c):
-        if m < 2:
-            return own[m].at[chunk_of(m, of, c), pl.ds(starts[r], parts[r])]
-        return own[m].at[pl.ds(starts[r], parts[r]), chunk_of(m, of, c)]
+        return own[m].at[window(m, of, c, starts[r], parts[r])]
 
     def place(m, slot, r, of, c):
-        if m < 2:
-            return full[m].at[slot, chunk_of(m, of, c), pl.ds(0, parts[r])]
-        return full[m].at[slot, pl.ds(0, parts[r]), chunk_of(m, of, c)]
+        return full[m].at[(slot,) + window(m, of, c, 0, parts[r])]
 
     IN_ACROSS, IN_BEYOND, IN_MATE, IN_RELAY, OUT_MATE, OUT_MIRROR, OUT_REST = range(7)
 
@@ -244,7 +246,7 @@
         return remote(src, place(m, slot, r, of, c), z_send.at[m, lane, c], arrive, {"sp": to})
 
     def ship_all(kind, m):
-        for c in range(SPLIT):
+        for c in range(PIECES):
             ship(kind, m, c).start()
 
     def direct(m, slot, r):
@@ -254,9 +256,12 @@
         return remote(place(m, slot, r, g, c), place(m, slot, r, g, c), y_send.at[m, slot, c], y_recv.at[m, slot, c],
                       {"grp": 1 - g})
 
+    def pieces_of(m, cs):
+        return range(PIECES) if m < 2 else [c * deep + d for c in cs for d in range(deep)]
+
     def take(m, slot, cs=range(SPLIT)):
         def run(r):
-            for c in cs:
+            for c in pieces_of(m, cs):
                 remote(place(m, slot, r, g, c), place(m, slot, r, g, c), z_send.at[m, 0, c], z_recv.at[m, slot, c],
                        {"sp": mate}).wait_recv()
                 if not direct(m, slot, r):
@@ -268,7 +273,7 @@
 
     def have(m, slot, cs=range(SPLIT)):
         def run(r):
-            for c in cs:
+            for c in pieces_of(m, cs):
                 ref = place(m, slot, r, 1 - g, c)
                 remote(ref, ref, y_send.at[m, slot, c], y_recv.at[m, slot, c], {"grp": 1 - g}).wait_recv()
 
@@ -409,15 +414,17 @@
 
     my_cols = pl.ds(pl.multiple_of(t * cols, 128), cols)
 
-    def norm_part(first, col):
-        return normed.at[pl.ds(first, tokens), pl.ds(pl.multiple_of(col * cols, 128), cols)]
-
-    def norm_copy(i, arrival=False):
+    def norm_part(first, col, c):
+        step = tokens // PIECES
+        return normed.at[pl.ds(pl.multiple_of(first + c * step, EDGE), step),
+                         pl.ds(pl.multiple_of(col * cols, 128), cols)]
+
+    def norm_copy(i, c, arrival=False):
         first = base if i == 0 and not arrival else other_base
         col = (t, t, t, chip_peer)[i] if not arrival else (t, chip_peer, core_peer, lax.rem(core_peer + 2, tps))[i]
         to = ({"sp": mate}, {"tp": chip_peer}, {"tp": core_peer}, {"tp": core_peer})[i]
-        ref = norm_part(first, col)
-        return remote(ref, ref, norm_send.at[i], norm_recv.at[i], to)
+        ref = norm_part(first, col, c)
+        return remote(ref, ref, norm_send.at[i, c], norm_recv.at[i, c], to)
 
     edge_from = pl.ds(pl.multiple_of(base + jnp.where(low, tokens - EDGE, 0), EDGE), EDGE)
     edge_over = pl.ds(pl.multiple_of(jnp.where(low, 0, EDGE + rows2), EDGE), EDGE)
@@ -444,32 +451,40 @@
     with_edge = pl.ds(pl.multiple_of(jnp.where(low, EDGE, 0), EDGE), rows2 + EDGE)
     both = pl.ds(EDGE, rows2)
 
-    def gate_up(slot):
+    def gate_of(slot):
         if slot != OWN:
             have(0, slot)
-            have(1, slot)
         k = pl.ds(pl.multiple_of(source_of(slot) * depth, 128), depth)
 
         @pl.loop(0, my_part // tile)
         def _(i):
             at = pl.ds(pl.multiple_of(i * tile, 128), tile)
             ga = jnp.dot(normed[with_edge, k], wg_all[slot, :, at], preferred_element_type=F32)
-            if slot == OWN:
-                gate[with_edge, at] = ga
+            gate[with_edge, at] = ga if slot == OWN else gate[with_edge, at] + ga
+
+    def up_of(slot, last=False):
+        if slot != OWN:
+            have(1, slot)
+        k = pl.ds(pl.multiple_of(source_of(slot) * depth, 128), depth)
+
+        @pl.loop(0, my_part // tile)
+        def _(i):
+            at = pl.ds(pl.multiple_of(i * tile, 128), tile)
+            ub = jnp.dot(normed[both, k], wu_all[slot, :, at], preferred_element_type=F32)
+            if slot != OWN:
+                ub = up[:, at] + ub
+            if last:
+                act[:, at] = (silu[:, at] * ub.astype(BF16).astype(F32)).astype(BF16)
             else:
-                gate[with_edge, at] += ga
-            ub = jnp.dot(normed[both, k], wu_all[slot, :, at], preferred_element_type=F32)
-            if slot == OWN:
                 up[:, at] = ub
-            else:
-                up[:, at] += ub
 
     @pl.when(inner)
     def _():
         for i in range(2):
             edge_copy(i).start()
 
-    norm_copy(0).start()
+    for c in range(PIECES):
+        norm_copy(0, c).start()
 
     @pl.when(outer)
     def _():
@@ -495,41 +510,36 @@
     def _():
         take(1, 2)
 
-    norm_copy(0, True).wait_recv()
-    norm_copy(1).start()
-    norm_copy(2).start()
+    for c in range(PIECES):
+        norm_copy(0, c, True).wait_recv()
+        norm_copy(1, c).start()
+        norm_copy(2, c).start()
     edge_arrival().wait_recv()
     for j in range(1, tps):
         row_copy(j).start()
 
-    @pl.when(inner)
-    def _():
-        take(1, 1)
-
-    norm_copy(1, True).wait_recv()
-    norm_copy(3).start()
+    for c in range(PIECES):
+        norm_copy(1, c, True).wait_recv()
+        norm_copy(3, c).start()
 
     @pl.when(outer)
     def _():
         take(1, 2)
 
-    norm_copy(2, True).wait_recv()
-    norm_copy(3, True).wait_recv()
+    for c in range(PIECES):
+        norm_copy(2, c, True).wait_recv()
+        norm_copy(3, c, True).wait_recv()
     for j in range(1, tps):
         row_copy(j, True).wait_recv()
-    gate_up(OWN)
-    gate_up(0)
-
-    @pl.when(outer)
+    gate_of(OWN)
+    gate_of(0)
+    gate_of(2)
+    gate_of(1)
+
+    @pl.when(inner)
     def _():
         take(1, 1)
 
-    gate_up(2)
-
-    take(2, 0)
-
-    gate_up(1)
-
     @pl.when(low)
     def _():
         gate[0:EDGE, :] = jnp.zeros((EDGE, parts[0]), F32)
@@ -537,25 +547,33 @@
     @pl.when(jnp.logical_not(low))
     def _():
         gate[EDGE + rows2:, :] = jnp.zeros((EDGE, parts[0]), F32)
-
-    @pl.when(outer)
-    def _():
-        ship_all(OUT_MIRROR, 2)
-
-    @pl.when(inner)
-    def _():
-        take(2, 1, (0,))
 
     @pl.loop(0, my_part // 128)
     def _(i):
         at = pl.ds(pl.multiple_of(i * 128, 128), 128)
         ch = pl.ds(pl.multiple_of(hidden_at + i * 128, 128), 128)
         gate[:, at] = gate[:, at].astype(BF16).astype(F32)
-        conv = cb_ref[:, ch]
+        conv = cb_ref[pl.ds(role * (parts[0] // 128) + i, 1), :]
         for tap in range(CONV):
             conv = conv + gate[pl.ds(EDGE - CONV // 2 + tap, rows2), at] * cw_ref[tap:tap + 1, ch]
-        silu = conv / (1.0 + jnp.exp(-conv))
-        act[:, at] = (silu * up[:, at].astype(BF16).astype(F32)).astype(BF16)
+        silu[:, at] = conv / (1.0 + jnp.exp(-conv))
+
+    up_of(OWN)
+    up_of(0)
+    up_of(2)
+
+    @pl.when(outer)
+    def _():
+        ship_all(OUT_MIRROR, 2)
+        take(1, 1)
+
+    take(2, 0)
+
+    up_of(1, last=True)
+
+    @pl.when(inner)
+    def _():
+        take(2, 1, (0,))
 
     half_rows = tokens // 2
     wide = cols // SPLIT
@@ -594,6 +612,16 @@
     def far_copy(p, c):
         return remote(terms.at[p, half_of(1, core), block_of(c)], far_in.at[half_rows_of(core), block_of(c)],
                       far_send.at[lax.rem(p, 2), c], far_recv.at[core, c], {"tp": p})
+
+    def over_copy(slot, c):
+        p = source_of(slot)
+        to = {"tp": p} if slot == 1 else {"sp": mate, "tp": p}
+        return remote(terms.at[p, half_of(0, core), block_of(c)], over_in.at[half_rows_of(core), block_of(c)],
+                      over_send.at[slot - 1, c], over_recv.at[core, c], to)
+
+    def over_arrival(h, c):
+        ref = over_in.at[half_rows_of(h), block_of(c)]
+        return remote(ref, ref, over_send.at[0, c], over_recv.at[h, c], {"sp": mate, "tp": far_first + h})
 
     def far_arrival(h, c):
         ref = far_in.at[half_rows_of(h), block_of(c)]
@@ -619,7 +647,7 @@
         def _():
             pair_copy(p, i, c).start()
 
-    def gather(p, c):
+    def gather(p, c, late=None):
         for i in range(2):
             @pl.when(is_far(p))
             def _():
@@ -628,17 +656,42 @@
                 total = (terms[p, rows, block_of(c)].astype(F32)
                          + pair_in[lax.rem(p, 2), i, :, block_of(c)].astype(F32))
                 terms[p, rows, block_of(c)] = total.astype(BF16)
-                if i == 0:
+                if i == 0 and late:
+                    @pl.when(inner)
+                    def _():
+                        over_copy(late, c).start()
+
+                    @pl.when(outer)
+                    def _():
+                        mid_copy(p, c).start()
+                elif i == 0:
                     mid_copy(p, c).start()
 
-        @pl.when(p == t)
+        @pl.when((p == t) & outer if late == 1 else p == t)
         def _():
             near_copy(0, c).wait_recv()
             ret_out[:, block_of(c)] = (terms[t, rows_of(0), block_of(c)].astype(F32)
                                        + near_in[0, :, block_of(c)].astype(F32)).astype(BF16)
             ret_copy(c).start()
 
-    def send_far(p, c):
+    def ret_late(c):
+        @pl.when(inner & (t == source_of(1)))
+        def _():
+            near_copy(0, c).wait_recv()
+            for h in range(2):
+                over_arrival(h, c).wait_recv()
+            ret_out[:, block_of(c)] = (terms[t, rows_of(0), block_of(c)].astype(F32)
+                                       + near_in[0, :, block_of(c)].astype(F32)
+                                       + over_in[:, block_of(c)].astype(F32)).astype(BF16)
+            ret_copy(c).start()
+
+    def send_far(p, c, last=False):
+        if last:
+            @pl.when(is_far(p))
+            def _():
+                far_copy(p, c).start()
+            return
+
         @pl.when(is_far(p))
         def _():
             mid_copy(p, c).wait_recv()
@@ -659,9 +712,57 @@
         out = out + ret_in[:, block_of(c)].astype(F32)
         out_ref[:, block_of(c)] = out.astype(BF16)
 
+        @pl.when(outer & (t == source_of(2)))
+        def _():
+            for h in range(2):
+                over_arrival(h, c).wait_recv()
+            out_ref[:, block_of(c)] = (out + over_in[:, block_of(c)].astype(F32)).astype(BF16)
+
     def downs(slot, p, c):
         for i in range(2):
             down(slot, p, c, i)
+
+    def drain(ms):
+        def run(r):
+            for kind in ((IN_ACROSS, IN_BEYOND, IN_MATE, IN_RELAY), (OUT_MATE, OUT_MIRROR, OUT_REST))[r]:
+                for m in ms:
+                    for c in range(PIECES):
+                        if m == 2 or kind != OUT_REST:
+                            ship(kind, m, c).wait_send()
+            for m in ms:
+                for slot in range(n - 1):
+                    for c in range(PIECES):
+                        if not direct(m, slot, r):
+                            cross(m, slot, r, c).wait_send()
+
+        by_role(run)
+
+    def drain_first():
+        drain((0, 1))
+        for i in range(4):
+            for c in range(PIECES):
+                norm_copy(i, c).wait_send()
+        for j in range(1, tps):
+            row_copy(j).wait_send()
+
+        @pl.when(inner)
+        def _():
+            for i in range(2):
+                edge_copy(i).wait_send()
+
+        @pl.when(has_left)
+        def _():
+            for i in range(2):
+                halo_copy(i, True).wait_send()
+
+        @pl.when(has_right)
+        def _():
+            for i in range(2):
+                halo_copy(i, False).wait_send()
+
+        for step in range(3):
+            spread(*proj_args, step).wait_send()
+            spread(*mix_args, step).wait_send()
 
     have(2, 0)
     early = [(jnp.where(inner, OWN, 0), jnp.where(inner, s, mate)), (jnp.where(inner, 0, OWN), jnp.where(inner, mate, s))]
@@ -683,71 +784,59 @@
             have(2, slot, (c,))
         downs(slot, p, c)
         if at >= head:
-            gather(p, c)
+            gather(p, c, slot)
+            if slot == 2:
+                ret_late(c)
             send_far(*steps[at - head][1:])
-            if at > head:
-                send_far(*steps[at - 1][1:])
+            if at == head:
+                drain_first()
+
+            @pl.when(inner)
+            def _():
+                for late_at in {head: (), head + 1: (head, head + 1)}.get(at, (at,)):
+                    send_far(*steps[late_at][1:])
+
+            @pl.when(outer)
+            def _():
+                send_far(p, c, True)
         elif at:
             gather(*steps[at - 1][1:])
-    send_far(*steps[-1][1:])
+
+    drain((2,))
     for c in range(SPLIT):
-        finish(c)
-
-    @pl.when(inner)
-    def _():
-        for kind in (IN_ACROSS, IN_BEYOND, IN_MATE, IN_RELAY):
-            for m in range(3):
-                for c in range(SPLIT):
-                    ship(kind, m, c).wait_send()
-
-    @pl.when(outer)
-    def _():
-        for kind in (OUT_MATE, OUT_MIRROR, OUT_REST):
-            for m in range(3) if kind != OUT_REST else (2,):
-                for c in range(SPLIT):
-                    ship(kind, m, c).wait_send()
-
-    def crossed(r):
-        for m in range(3):
-            for slot in range(n - 1):
-                for c in range(SPLIT):
-                    if not direct(m, slot, r):
-                        cross(m, slot, r, c).wait_send()
-
-    by_role(crossed)
-    for i in range(4):
-        norm_copy(i).wait_send()
-    for j in range(1, tps):
-        row_copy(j).wait_send()
-
-    @pl.when(inner)
-    def _():
-        for i in range(2):
-            edge_copy(i).wait_send()
-
-    for c in range(SPLIT):
-        ret_copy(c).wait_send()
         for i in range(2):
             near_copy(i, c).wait_send()
             for h in range(2):
                 pair_copy(far_first + h, i, c).wait_send()
-        for h in range(2):
-            mid_copy(far_first + h, c).wait_send()
-            far_copy(far_first + h, c).wait_send()
-
-    @pl.when(has_left)
-    def _():
-        for i in range(2):
-            halo_copy(i, True).wait_send()
-
-    @pl.when(has_right)
-    def _():
-        for i in range(2):
-            halo_copy(i, False).wait_send()
-
-    for step in range(3):
-        spread(*proj_args, step).wait_send()
-        spread(*mix_args, step).wait_send()
+
+    def mids(here, owners):
+        @pl.when(here)
+        def _():
+            for c in range(SPLIT):
+                for p in owners:
+                    @pl.when(is_far(p))
+                    def _():
+                        mid_copy(p, c).wait_send()
+
+    mids(inner, [p for _, p, c in early if c == 0])
+    mids(outer, [p for _, p, c in steps if c == 0])
+
+    @pl.when(inner)
+    def _():
+        for slot in (1, 2):
+            @pl.when(is_far(source_of(slot)))
+            def _():
+                for c in range(SPLIT):
+                    over_copy(slot, c).wait_send()
+
+    finish(0)
+    ret_copy(0).wait_send()
+    for h in range(2):
+        far_copy(far_first + h, 0).wait_send()
+    finish(1)
+    ret_copy(1).wait_send()
+    for h in range(2):
+        far_copy(far_first + h, 1).wait_send()
 
 
 def kernel_shards(
@@ -781,6 +870,7 @@
             pltpu.VMEM((n, part, cols), BF16),
             pltpu.VMEM((2 * tokens + 2 * EDGE, part), F32),
             pltpu.VMEM((2 * tokens, part), F32),
+            pltpu.VMEM((2 * tokens, part), F32),
             pltpu.VMEM((2 * tokens, part), BF16),
             pltpu.VMEM((tps, 2 * tokens, cols), BF16),
             pltpu.VMEM((2,) + block, BF16),
@@ -789,23 +879,25 @@
             pltpu.VMEM((2, tokens // 2, cols), BF16),
             pltpu.VMEM(block, BF16),
             pltpu.VMEM(block, BF16),
+            pltpu.VMEM(block, BF16),
             dma((8,)), dma((2, 2)), dma((2, 2)),
-            dma((3, 4, SPLIT)), dma((3, 3, SPLIT)), dma((3, 3, SPLIT)), dma((3, 3, SPLIT)),
-            dma((3,)), dma((3,)), dma((3,)), dma((3,)), dma((4,)), dma((4,)), dma((2,)), dma((1,)),
+            dma((3, 4, PIECES)), dma((3, 3, PIECES)), dma((3, 3, PIECES)), dma((3, 3, PIECES)),
+            dma((3,)), dma((3,)), dma((3,)), dma((3,)), dma((4, PIECES)), dma((4, PIECES)), dma((2,)), dma((1,)),
             dma((3,)), dma((3,)),
             dma((2, SPLIT)), dma((2, SPLIT)), dma((2, 2, SPLIT)), dma((2, 2, SPLIT)),
-            dma((2, SPLIT)), dma((2, SPLIT)), dma((2, SPLIT)), dma((2, SPLIT)), dma((SPLIT,)), dma((SPLIT,)),
+            dma((2, SPLIT)), dma((2, SPLIT)), dma((2, SPLIT)), dma((2, SPLIT)),
+            dma((2, SPLIT)), dma((2, SPLIT)), dma((SPLIT,)), dma((SPLIT,)),
         ],
         compiler_params=pltpu.CompilerParams(
             collective_id=0, has_side_effects=True, vmem_limit_bytes=67043328
         ),
-    )(queries, keys, values, sink, resid, out_proj, norm_gain[None], w_gate, w_up, conv_w, conv_b[None], w_down)
+    )(queries, keys, values, sink, resid, out_proj, norm_gain[None], w_gate, w_up, conv_w, conv_b.reshape(hidden // 128, 128), w_down)
 
 
 def fits_kernel(sizes, args):
     groups, n, tps = sizes
     queries, resid, out_proj, w_gate, w_down = args[0], args[4], args[5], args[7], args[11]
-    share = groups * SPLIT
+    share = groups * PIECES
     weights = 3 * 2 * n * w_gate.shape[0] * w_gate.shape[1]
     return (
         n == 4
@@ -813,7 +905,7 @@
         and groups == 2
         and w_down.shape[1] == out_proj.shape[1]
         and w_gate.shape[0] % max(share * EDGE, 128) == 0
-        and w_down.shape[1] % (share * 128) == 0
+        and w_down.shape[1] % (groups * SPLIT * 128) == 0
         and w_gate.shape[1] % 768 == 0
         and resid.shape[0] % (4 * WINDOW) == 0
         and weights <= 20 * 2 ** 20

time: 134 us -> 129 us (0.963)
  Pallas kernels: 131 us -> 127 us
    pallas_call x1, Pallas kernels: 131 us -> 127 us  [kernel_shards(): pl.pallas_call(functools.partial(layer_kernel, sizes), out_shape=jax.Shap...]
where the time goes in v3:
time: 129 us; the launch traced here: 128 us
  Pallas kernels  127 us (98%)
  local copies, waits for them, and re-layouts  1.87 us (1%)
    pallas_call x1, Pallas kernels, kernel_shards(): pl.pallas_call(functools.partial(layer_kernel, sizes), out_shape=jax.Shap...  127 us

profile of v3, /device:TPU:16, one launch (start us, length us, event | category | flops | bytes accessed | tf_op | source)
XLA Modules:
  0.0 128.5 jit_solution(2972729216644798593)
XLA Ops:
  0.0 126.6 %shard_map.118 = bf16[512,512]{1,0:T(8,128)(2,1)} custom-call(bf16[512,256]{1,0:T(8,128)(2,1)} %q_hbm.1, bf16[512,256]{1,0:T(8,128)(2,1)} %k_hbm.1, bf16[512,256]{1,0:T(8,128)(2,1)} %v_hbm.1, f32[2]{0:T(128)} %sink_ref.1, bf16[512,2048]{1,0:T(8,128)(2,1)} %resid_hbm.1, bf16[1024,512]{1,0:T(8,128)(2,1)} %proj_hbm.1, f32[1,2048]{1,0:T(1,128)} %bitcast.2, ...), custom_call_target="tpu_custom_call" | custom-call | tf_op jit(solution)/shard_map/pallas_call | solution.py:855
  126.6 1.9 %copy.14 = bf16[512,512]{1,0:T(8,128)(2,1)} copy(bf16[512,512]{1,0:T(8,128)(2,1)} %shard_map.118) | data formatting | bytes 1048576

commit v4 on v3

--- a/solution.py
+++ b/solution.py
@@ -243,7 +243,7 @@
         of = 1 - g if kind == OUT_REST else g
         src = place(m, 0, r, of, c) if kind == IN_RELAY else source(m, r, of, c)
         arrive = y_recv.at[m, slot, c] if kind == OUT_REST else z_recv.at[m, slot, c]
-        return remote(src, place(m, slot, r, of, c), z_send.at[m, lane, c], arrive, {"sp": to})
+        return remote(src, place(m, slot, r, of, c), z_send.at[m, lane], arrive, {"sp": to})
 
     def ship_all(kind, m):
         for c in range(PIECES):
@@ -253,8 +253,23 @@
         return r == 0 and m == 2 and isinstance(slot, int) and slot == 0
 
     def cross(m, slot, r, c):
-        return remote(place(m, slot, r, g, c), place(m, slot, r, g, c), y_send.at[m, slot, c], y_recv.at[m, slot, c],
+        return remote(place(m, slot, r, g, c), place(m, slot, r, g, c), y_send.at[m, slot], y_recv.at[m, slot, c],
                       {"grp": 1 - g})
+
+    def share_of(m, r):
+        if m < 2:
+            return full[m].at[0, pl.ds(0, depth // groups), pl.ds(0, parts[r])]
+        return full[m].at[0, pl.ds(0, parts[r]), pl.ds(0, cols // groups)]
+
+    def shipped(kind, m):
+        r = 0 if kind in (IN_ACROSS, IN_RELAY, OUT_MATE, OUT_REST) else 1
+        lane = {IN_BEYOND: 1, IN_MATE: 2, IN_RELAY: 3, OUT_MIRROR: 1, OUT_REST: 2}.get(kind, 0)
+        ref = share_of(m, r)
+        remote(ref, ref, z_send.at[m, lane], z_recv.at[m, 0, 0], {"sp": mate}).wait_send()
+
+    def crossed(m, slot, r):
+        ref = share_of(m, r)
+        remote(ref, ref, y_send.at[m, slot], y_recv.at[m, slot, 0], {"grp": 1 - g}).wait_send()
 
     def pieces_of(m, cs):
         return range(PIECES) if m < 2 else [c * deep + d for c in cs for d in range(deep)]
@@ -262,7 +277,7 @@
     def take(m, slot, cs=range(SPLIT)):
         def run(r):
             for c in pieces_of(m, cs):
-                remote(place(m, slot, r, g, c), place(m, slot, r, g, c), z_send.at[m, 0, c], z_recv.at[m, slot, c],
+                remote(place(m, slot, r, g, c), place(m, slot, r, g, c), z_send.at[m, 0], z_recv.at[m, slot, c],
                        {"sp": mate}).wait_recv()
                 if not direct(m, slot, r):
                     cross(m, slot, r, c).start()
@@ -275,7 +290,7 @@
         def run(r):
             for c in pieces_of(m, cs):
                 ref = place(m, slot, r, 1 - g, c)
-                remote(ref, ref, y_send.at[m, slot, c], y_recv.at[m, slot, c], {"grp": 1 - g}).wait_recv()
+                remote(ref, ref, y_send.at[m, slot], y_recv.at[m, slot, c], {"grp": 1 - g}).wait_recv()
 
         by_role(run)
 
@@ -424,7 +439,7 @@
         col = (t, t, t, chip_peer)[i] if not arrival else (t, chip_peer, core_peer, lax.rem(core_peer + 2, tps))[i]
         to = ({"sp": mate}, {"tp": chip_peer}, {"tp": core_peer}, {"tp": core_peer})[i]
         ref = norm_part(first, col, c)
-        return remote(ref, ref, norm_send.at[i, c], norm_recv.at[i, c], to)
+        return remote(ref, ref, norm_send.at[i], norm_recv.at[i, c], to)
 
     edge_from = pl.ds(pl.multiple_of(base + jnp.where(low, tokens - EDGE, 0), EDGE), EDGE)
     edge_over = pl.ds(pl.multiple_of(jnp.where(low, 0, EDGE + rows2), EDGE), EDGE)
@@ -726,22 +741,20 @@
         def run(r):
             for kind in ((IN_ACROSS, IN_BEYOND, IN_MATE, IN_RELAY), (OUT_MATE, OUT_MIRROR, OUT_REST))[r]:
                 for m in ms:
-                    for c in range(PIECES):
-                        if m == 2 or kind != OUT_REST:
-                            ship(kind, m, c).wait_send()
+                    if m == 2 or kind != OUT_REST:
+                        shipped(kind, m)
             for m in ms:
                 for slot in range(n - 1):
-                    for c in range(PIECES):
-                        if not direct(m, slot, r):
-                            cross(m, slot, r, c).wait_send()
+                    if not direct(m, slot, r):
+                        crossed(m, slot, r)
 
         by_role(run)
 
     def drain_first():
         drain((0, 1))
         for i in range(4):
-            for c in range(PIECES):
-                norm_copy(i, c).wait_send()
+            ref = normed.at[pl.ds(EDGE, tokens), pl.ds(0, cols)]
+            remote(ref, ref, norm_send.at[i], norm_recv.at[i, 0], {"sp": mate}).wait_send()
         for j in range(1, tps):
             row_copy(j).wait_send()
 
@@ -785,15 +798,15 @@
         downs(slot, p, c)
         if at >= head:
             gather(p, c, slot)
-            if slot == 2:
-                ret_late(c)
+            if at in (head + 1, head + 2):
+                ret_late(at - head - 1)
             send_far(*steps[at - head][1:])
             if at == head:
                 drain_first()
 
             @pl.when(inner)
             def _():
-                for late_at in {head: (), head + 1: (head, head + 1)}.get(at, (at,)):
+                for late_at in {head: (), head + 1: (head,), head + 2: (head + 1, head + 2)}.get(at, (at,)):
                     send_far(*steps[late_at][1:])
 
             @pl.when(outer)
@@ -881,8 +894,8 @@
             pltpu.VMEM(block, BF16),
             pltpu.VMEM(block, BF16),
             dma((8,)), dma((2, 2)), dma((2, 2)),
-            dma((3, 4, PIECES)), dma((3, 3, PIECES)), dma((3, 3, PIECES)), dma((3, 3, PIECES)),
-            dma((3,)), dma((3,)), dma((3,)), dma((3,)), dma((4, PIECES)), dma((4, PIECES)), dma((2,)), dma((1,)),
+            dma((3, 4)), dma((3, 3, PIECES)), dma((3, 3)), dma((3, 3, PIECES)),
+            dma((3,)), dma((3,)), dma((3,)), dma((3,)), dma((4,)), dma((4, PIECES)), dma((2,)), dma((1,)),
             dma((3,)), dma((3,)),
             dma((2, SPLIT)), dma((2, SPLIT)), dma((2, 2, SPLIT)), dma((2, 2, SPLIT)),
             dma((2, SPLIT)), dma((2, SPLIT)), dma((2, SPLIT)), dma((2, SPLIT)),

time: 129 us -> 126 us (0.977)
  Pallas kernels: 127 us -> 124 us
    pallas_call x1, Pallas kernels: 127 us -> 124 us  [kernel_shards(): pl.pallas_call(functools.partial(layer_kernel, sizes), out_shape=jax.Shap...]
where the time goes in v4:
time: 126 us
  Pallas kernels  124 us (98%)
  local copies, waits for them, and re-layouts  1.87 us (1%)
    pallas_call x1, Pallas kernels, kernel_shards(): pl.pallas_call(functools.partial(layer_kernel, sizes), out_shape=jax.Shap...  124 us

profile of v4, /device:TPU:16, one launch (start us, length us, event | category | flops | bytes accessed | tf_op | source)
XLA Modules:
  0.0 125.9 jit_solution(15512030476498874791)
XLA Ops:
  0.0 124.0 %shard_map.118 = bf16[512,512]{1,0:T(8,128)(2,1)} custom-call(bf16[512,256]{1,0:T(8,128)(2,1)} %q_hbm.1, bf16[512,256]{1,0:T(8,128)(2,1)} %k_hbm.1, bf16[512,256]{1,0:T(8,128)(2,1)} %v_hbm.1, f32[2]{0:T(128)} %sink_ref.1, bf16[512,2048]{1,0:T(8,128)(2,1)} %resid_hbm.1, bf16[1024,512]{1,0:T(8,128)(2,1)} %proj_hbm.1, f32[1,2048]{1,0:T(1,128)} %bitcast.2, ...), custom_call_target="tpu_custom_call" | custom-call | tf_op jit(solution)/shard_map/pallas_call | solution.py:868
  124.1 1.9 %copy.14 = bf16[512,512]{1,0:T(8,128)(2,1)} copy(bf16[512,512]{1,0:T(8,128)(2,1)} %shard_map.118) | data formatting | bytes 1048576

commit v5 on v4

--- a/solution.py
+++ b/solution.py
@@ -105,7 +105,8 @@
 
 EDGE = 16
 SPLIT = 2
-PIECES = 4
+PIECES = 2
+DEEP = 8
 BF16 = jnp.bfloat16
 F32 = jnp.float32
 
@@ -211,7 +212,13 @@
         return remote(ref.at[pl.ds(tokens - WINDOW, WINDOW), kv_cols], kv_ext.at[i, pl.ds(0, WINDOW)],
                       halo_send.at[i, 1], halo_recv.at[i, 1], {"sp": s + 1})
 
-    deep = PIECES // SPLIT
+    deep = DEEP // SPLIT
+
+    def count_of(m):
+        return PIECES if m < 2 else DEEP
+
+    def landing(sems, m, slot, c):
+        return sems.at[(m * (n - 1) + slot) * PIECES + c if m < 2 else 2 * (n - 1) * PIECES + slot * DEEP + c]
 
     def window(m, of, c, first, count):
         if m < 2:
@@ -242,18 +249,18 @@
         r = 0 if kind in (IN_ACROSS, IN_RELAY, OUT_MATE, OUT_REST) else 1
         of = 1 - g if kind == OUT_REST else g
         src = place(m, 0, r, of, c) if kind == IN_RELAY else source(m, r, of, c)
-        arrive = y_recv.at[m, slot, c] if kind == OUT_REST else z_recv.at[m, slot, c]
+        arrive = landing(y_recv, m, slot, c) if kind == OUT_REST else landing(z_recv, m, slot, c)
         return remote(src, place(m, slot, r, of, c), z_send.at[m, lane], arrive, {"sp": to})
 
     def ship_all(kind, m):
-        for c in range(PIECES):
+        for c in range(count_of(m)):
             ship(kind, m, c).start()
 
     def direct(m, slot, r):
         return r == 0 and m == 2 and isinstance(slot, int) and slot == 0
 
     def cross(m, slot, r, c):
-        return remote(place(m, slot, r, g, c), place(m, slot, r, g, c), y_send.at[m, slot], y_recv.at[m, slot, c],
+        return remote(place(m, slot, r, g, c), place(m, slot, r, g, c), y_send.at[m, slot], landing(y_recv, m, slot, c),
                       {"grp": 1 - g})
 
     def share_of(m, r):
@@ -265,11 +272,11 @@
         r = 0 if kind in (IN_ACROSS, IN_RELAY, OUT_MATE, OUT_REST) else 1
         lane = {IN_BEYOND: 1, IN_MATE: 2, IN_RELAY: 3, OUT_MIRROR: 1, OUT_REST: 2}.get(kind, 0)
         ref = share_of(m, r)
-        remote(ref, ref, z_send.at[m, lane], z_recv.at[m, 0, 0], {"sp": mate}).wait_send()
+        remote(ref, ref, z_send.at[m, lane], landing(z_recv, m, 0, 0), {"sp": mate}).wait_send()
 
     def crossed(m, slot, r):
         ref = share_of(m, r)
-        remote(ref, ref, y_send.at[m, slot], y_recv.at[m, slot, 0], {"grp": 1 - g}).wait_send()
+        remote(ref, ref, y_send.at[m, slot], landing(y_recv, m, slot, 0), {"grp": 1 - g}).wait_send()
 
     def pieces_of(m, cs):
         return range(PIECES) if m < 2 else [c * deep + d for c in cs for d in range(deep)]
@@ -277,7 +284,7 @@
     def take(m, slot, cs=range(SPLIT)):
         def run(r):
             for c in pieces_of(m, cs):
-                remote(place(m, slot, r, g, c), place(m, slot, r, g, c), z_send.at[m, 0], z_recv.at[m, slot, c],
+                remote(place(m, slot, r, g, c), place(m, slot, r, g, c), z_send.at[m, 0], landing(z_recv, m, slot, c),
                        {"sp": mate}).wait_recv()
                 if not direct(m, slot, r):
                     cross(m, slot, r, c).start()
@@ -290,7 +297,7 @@
         def run(r):
             for c in pieces_of(m, cs):
                 ref = place(m, slot, r, 1 - g, c)
-                remote(ref, ref, y_send.at[m, slot], y_recv.at[m, slot, c], {"grp": 1 - g}).wait_recv()
+                remote(ref, ref, y_send.at[m, slot], landing(y_recv, m, slot, c), {"grp": 1 - g}).wait_recv()
 
         by_role(run)
 
@@ -554,6 +561,7 @@
     @pl.when(inner)
     def _():
         take(1, 1)
+        take(2, 0)
 
     @pl.when(low)
     def _():
@@ -573,6 +581,10 @@
             conv = conv + gate[pl.ds(EDGE - CONV // 2 + tap, rows2), at] * cw_ref[tap:tap + 1, ch]
         silu[:, at] = conv / (1.0 + jnp.exp(-conv))
 
+    @pl.when(outer)
+    def _():
+        take(2, 0)
+
     up_of(OWN)
     up_of(0)
     up_of(2)
@@ -582,7 +594,6 @@
         ship_all(OUT_MIRROR, 2)
         take(1, 1)
 
-    take(2, 0)
 
     up_of(1, last=True)
 
@@ -894,7 +905,7 @@
             pltpu.VMEM(block, BF16),
             pltpu.VMEM(block, BF16),
             dma((8,)), dma((2, 2)), dma((2, 2)),
-            dma((3, 4)), dma((3, 3, PIECES)), dma((3, 3)), dma((3, 3, PIECES)),
+            dma((3, 4)), dma((6 * PIECES + 3 * DEEP,)), dma((3, 3)), dma((6 * PIECES + 3 * DEEP,)),
             dma((3,)), dma((3,)), dma((3,)), dma((3,)), dma((4,)), dma((4, PIECES)), dma((2,)), dma((1,)),
             dma((3,)), dma((3,)),
             dma((2, SPLIT)), dma((2, SPLIT)), dma((2, 2, SPLIT)), dma((2, 2, SPLIT)),

time: 126 us -> 126 us (level)
  no operation moved by 1% of the time
where the time goes in v5:
time: 126 us
  Pallas kernels  124 us (98%)
  local copies, waits for them, and re-layouts  1.87 us (1%)
    pallas_call x1, Pallas kernels, kernel_shards(): pl.pallas_call(functools.partial(layer_kernel, sizes), out_shape=jax.Shap...  124 us

profile of v5, /device:TPU:16, one launch (start us, length us, event | category | flops | bytes accessed | tf_op | source)
XLA Modules:
  0.0 125.9 jit_solution(5677681509048317515)
XLA Ops:
  0.0 124.0 %shard_map.118 = bf16[512,512]{1,0:T(8,128)(2,1)} custom-call(bf16[512,256]{1,0:T(8,128)(2,1)} %q_hbm.1, bf16[512,256]{1,0:T(8,128)(2,1)} %k_hbm.1, bf16[512,256]{1,0:T(8,128)(2,1)} %v_hbm.1, f32[2]{0:T(128)} %sink_ref.1, bf16[512,2048]{1,0:T(8,128)(2,1)} %resid_hbm.1, bf16[1024,512]{1,0:T(8,128)(2,1)} %proj_hbm.1, f32[1,2048]{1,0:T(1,128)} %bitcast.2, ...), custom_call_target="tpu_custom_call" | custom-call | tf_op jit(solution)/shard_map/pallas_call | solution.py:879
  124.0 1.9 %copy.14 = bf16[512,512]{1,0:T(8,128)(2,1)} copy(bf16[512,512]{1,0:T(8,128)(2,1)} %shard_map.118) | data formatting | bytes 1048576

commit v6 on v5

--- a/solution.py
+++ b/solution.py
@@ -217,6 +217,9 @@
     def count_of(m):
         return PIECES if m < 2 else DEEP
 
+    def crossing(m, slot, c):
+        return y_recv.at[m * (n - 1) + slot if m < 2 else 2 * (n - 1) + slot * SPLIT + c // deep]
+
     def landing(sems, m, slot, c):
         return sems.at[(m * (n - 1) + slot) * PIECES + c if m < 2 else 2 * (n - 1) * PIECES + slot * DEEP + c]
 
@@ -249,7 +252,7 @@
         r = 0 if kind in (IN_ACROSS, IN_RELAY, OUT_MATE, OUT_REST) else 1
         of = 1 - g if kind == OUT_REST else g
         src = place(m, 0, r, of, c) if kind == IN_RELAY else source(m, r, of, c)
-        arrive = landing(y_recv, m, slot, c) if kind == OUT_REST else landing(z_recv, m, slot, c)
+        arrive = crossing(m, slot, c) if kind == OUT_REST else landing(z_recv, m, slot, c)
         return remote(src, place(m, slot, r, of, c), z_send.at[m, lane], arrive, {"sp": to})
 
     def ship_all(kind, m):
@@ -260,7 +263,7 @@
         return r == 0 and m == 2 and isinstance(slot, int) and slot == 0
 
     def cross(m, slot, r, c):
-        return remote(place(m, slot, r, g, c), place(m, slot, r, g, c), y_send.at[m, slot], landing(y_recv, m, slot, c),
+        return remote(place(m, slot, r, g, c), place(m, slot, r, g, c), y_send.at[m, slot], crossing(m, slot, c),
                       {"grp": 1 - g})
 
     def share_of(m, r):
@@ -276,7 +279,7 @@
 
     def crossed(m, slot, r):
         ref = share_of(m, r)
-        remote(ref, ref, y_send.at[m, slot], landing(y_recv, m, slot, 0), {"grp": 1 - g}).wait_send()
+        remote(ref, ref, y_send.at[m, slot], crossing(m, slot, 0), {"grp": 1 - g}).wait_send()
 
     def pieces_of(m, cs):
         return range(PIECES) if m < 2 else [c * deep + d for c in cs for d in range(deep)]
@@ -295,9 +298,15 @@
 
     def have(m, slot, cs=range(SPLIT)):
         def run(r):
-            for c in pieces_of(m, cs):
-                ref = place(m, slot, r, 1 - g, c)
-                remote(ref, ref, y_send.at[m, slot], landing(y_recv, m, slot, c), {"grp": 1 - g}).wait_recv()
+            for c in cs if m == 2 else (0,):
+                if m < 2:
+                    step = depth // groups
+                    ref = full[m].at[slot, pl.ds(pl.multiple_of((1 - g) * step, EDGE), step), pl.ds(0, parts[r])]
+                else:
+                    step = cols // (groups * SPLIT)
+                    at = pl.multiple_of((c * groups + 1 - g) * step, 128)
+                    ref = full[m].at[slot, pl.ds(0, parts[r]), pl.ds(at, step)]
+                remote(ref, ref, y_send.at[m, slot], crossing(m, slot, c * deep), {"grp": 1 - g}).wait_recv()
 
         by_role(run)
 
@@ -905,7 +914,7 @@
             pltpu.VMEM(block, BF16),
             pltpu.VMEM(block, BF16),
             dma((8,)), dma((2, 2)), dma((2, 2)),
-            dma((3, 4)), dma((6 * PIECES + 3 * DEEP,)), dma((3, 3)), dma((6 * PIECES + 3 * DEEP,)),
+            dma((3, 4)), dma((6 * PIECES + 3 * DEEP,)), dma((3, 3)), dma((6 + 3 * SPLIT,)),
             dma((3,)), dma((3,)), dma((3,)), dma((3,)), dma((4,)), dma((4, PIECES)), dma((2,)), dma((1,)),
             dma((3,)), dma((3,)),
             dma((2, SPLIT)), dma((2, SPLIT)), dma((2, 2, SPLIT)), dma((2, 2, SPLIT)),

time: 126 us -> 126 us (level)
  no operation moved by 1% of the time
where the time goes in v6:
time: 126 us
  Pallas kernels  124 us (98%)
  local copies, waits for them, and re-layouts  1.87 us (1%)
    pallas_call x1, Pallas kernels, kernel_shards(): pl.pallas_call(functools.partial(layer_kernel, sizes), out_shape=jax.Shap...  124 us

profile of v6, /device:TPU:16, one launch (start us, length us, event | category | flops | bytes accessed | tf_op | source)
XLA Modules:
  0.0 125.6 jit_solution(4803423536253154931)
XLA Ops:
  0.0 123.8 %shard_map.118 = bf16[512,512]{1,0:T(8,128)(2,1)} custom-call(bf16[512,256]{1,0:T(8,128)(2,1)} %q_hbm.1, bf16[512,256]{1,0:T(8,128)(2,1)} %k_hbm.1, bf16[512,256]{1,0:T(8,128)(2,1)} %v_hbm.1, f32[2]{0:T(128)} %sink_ref.1, bf16[512,2048]{1,0:T(8,128)(2,1)} %resid_hbm.1, bf16[1024,512]{1,0:T(8,128)(2,1)} %proj_hbm.1, f32[1,2048]{1,0:T(1,128)} %bitcast.2, ...), custom_call_target="tpu_custom_call" | custom-call | tf_op jit(solution)/shard_map/pallas_call | solution.py:888
  123.8 1.9 %copy.14 = bf16[512,512]{1,0:T(8,128)(2,1)} copy(bf16[512,512]{1,0:T(8,128)(2,1)} %shard_map.118) | data formatting | bytes 1048576
